TPU v7x, 32 devices: a whole 2x2x4 slice. The times are simulated.
32 devices in a mesh: sp: 8 (over z, core), tp: 4 (over y, x).
Axes of the slice: x: 2, y: 2, z: 4, core: 2. Of those that a mesh axis runs over, the one named last changes fastest.
Arguments:
- receptance: bfloat16 [2048, 4096], P('sp', 'tp'), may hold values from -6 to 6
- key_vectors: bfloat16 [2048, 4096], P('sp', 'tp'), may hold values from -13 to 13
- value_vectors: bfloat16 [2048, 4096], P('sp', 'tp'), may hold values from -6 to 6
- decay_logits: bfloat16 [2048, 4096], P('sp', 'tp'), may hold values from -20 to 2
- rate_logits: bfloat16 [2048, 4096], P('sp', 'tp'), may hold values from -8 to 4
- gate_logits: bfloat16 [2048, 4096], P('sp', 'tp'), may hold values from -6 to 6
- group_gain: float32 [4096], P('tp'), may hold values from 0.1 to 1.9
- residual: bfloat16 [2048, 4096], P('sp', 'tp'), may hold values from -24 to 24
- mixer_out: bfloat16 [4096, 4096], P(None, 'tp'), may hold values from -0.09375 to 0.09375
- norm_gain: float32 [4096], P('tp'), may hold values from 0.1 to 1.9
- expert_ids: int32 [2048, 2], P('sp'), may hold values from 0 to 7, as said below
- route_weight: float32 [2048, 2], P('sp'), may hold values from 0.25 to 1
- expert_gate: bfloat16 [8, 4096, 1024], P('sp', 'tp'), may hold values from -0.09375 to 0.09375
- expert_up: bfloat16 [8, 4096, 1024], P('sp', 'tp'), may hold values from -0.09375 to 0.09375
- expert_down: bfloat16 [8, 1024, 4096], P('sp', None, 'tp'), may hold values from -0.1875 to 0.1875
Outputs:
- updated: bfloat16 [2048, 4096], P('sp', 'tp')
Inputs may be any that keep to these rules, and one draw needn't show every extreme that they name: `expert_ids`: the experts of a row are different and lie in one group of 2 consecutive experts. In the rows of one index of sp (aligned blocks of 256 rows) no expert is named by more than 128 rows, and in every such block some expert is named by exactly 128 rows.
All inputs are finite; a program needn't handle non-finite values.
Results may differ from a plain program's by a relative error of at most 0.013.
Values may be sent and summed in bfloat16 or wider, within the bound.
A program may use at most 128 MiB of HBM per device.

v0:
```python
import jax
import jax.numpy as jnp
from jax import lax
from jax.experimental import pallas as pl
from jax.experimental.pallas import tpu as pltpu
from jax.sharding import PartitionSpec as P

D = 4096
HEAD = 64
CHUNK = 128
EXP_HALF = 0.6065306597126334


EPS_GROUP = 0.00064
EPS_NORM = 1e-06


def split(x):
    hi = x.astype(jnp.bfloat16)
    lo = (x - hi.astype(jnp.float32)).astype(jnp.bfloat16)
    return hi, lo


def dot(a, b, dims):
    return lax.dot_general(a, b, (dims, ((), ())), preferred_element_type=jnp.float32)


NN = ((1,), (0,))
NT = ((1,), (1,))
TN = ((0,), (0,))


def dot3(a, b, dims=NN):
    return dot(a[0], b[0], dims) + (dot(a[0], b[1], dims) + dot(a[1], b[0], dims))


def dot2(a, b, dims=NN):
    return dot(a[0], b, dims) + dot(a[1], b, dims)


def sigmoid(x):
    return 1.0 / (1.0 + jnp.exp(-x))


def mix_kernel(r_ref, k_ref, v_ref, d_ref, a_ref, out_ref, state_ref):
    tokens = r_ref.shape[0]
    chunks = tokens // CHUNK
    row = lax.broadcasted_iota(jnp.int32, (CHUNK, CHUNK), 0)
    col = lax.broadcasted_iota(jnp.int32, (CHUNK, CHUNK), 1)
    strict = col < row
    causal = col <= row
    eye = jnp.where(col == row, 1.0, 0.0)
    ones_lower = jnp.where(causal, 1.0, 0.0).astype(jnp.bfloat16)
    low = lax.broadcasted_iota(jnp.int32, (CHUNK, 2 * HEAD), 1) < HEAD

    work = []
    for chunk in range(chunks):
        rows = pl.ds(chunk * CHUNK, CHUNK)
        recept = r_ref[rows, :].astype(jnp.float32)
        keyvec = k_ref[rows, :].astype(jnp.float32)
        logdec = -EXP_HALF * sigmoid(d_ref[rows, :].astype(jnp.float32))
        first, second = split(logdec)
        third = (logdec - first.astype(jnp.float32) - second.astype(jnp.float32)).astype(jnp.bfloat16)
        cum_in = dot(ones_lower, first, NN) + (
            dot(ones_lower, second, NN) + dot(ones_lower, third, NN)
        )
        cum_end = cum_in[CHUNK - 1 :, :]
        squares = keyvec * keyvec
        norms = jnp.where(
            low,
            jnp.sum(squares[:, :HEAD], axis=1, keepdims=True),
            jnp.sum(squares[:, HEAD:], axis=1, keepdims=True),
        )
        unit_key = keyvec * lax.rsqrt(1.0 + norms)
        correction = unit_key * sigmoid(a_ref[rows, :].astype(jnp.float32))
        growth = jnp.exp(-cum_in)
        tail = jnp.exp(cum_end - cum_in)
        r_scaled = recept * jnp.exp(cum_in)
        u_scaled = unit_key * jnp.exp(cum_in - logdec)
        queries = split(jnp.concatenate([u_scaled, r_scaled], axis=0))
        sources = split(jnp.concatenate([keyvec * growth, correction * growth], axis=0))
        tails = split(jnp.concatenate([keyvec * tail, -(correction * tail)], axis=0))
        keep = jnp.broadcast_to(jnp.exp(cum_end), (2 * HEAD, 2 * HEAD)).T
        values = v_ref[rows, :]
        for head in range(2):
            lanes = slice(head * HEAD, (head + 1) * HEAD)
            query = tuple(q[:, lanes] for q in queries)
            source = tuple(s[:, lanes] for s in sources)
            scores = dot3(query, source, NT)
            work.append(
                dict(
                    head=head,
                    chunk=chunk,
                    query=query,
                    tail=tuple(t[:, lanes] for t in tails),
                    keep=keep[lanes, :],
                    value=jnp.concatenate(
                        [values[:, lanes], jnp.zeros((CHUNK, HEAD), jnp.bfloat16)], axis=1
                    ),
                    key_both=split(
                        jnp.concatenate(
                            [
                                jnp.where(strict, scores[:CHUNK, :CHUNK], 0.0),
                                jnp.where(causal, scores[CHUNK:, :CHUNK], 0.0),
                            ],
                            axis=0,
                        )
                    ),
                    pull=jnp.where(strict, scores[:CHUNK, CHUNK:], 0.0),
                    corr_read=split(jnp.where(causal, scores[CHUNK:, CHUNK:], 0.0)),
                )
            )
    for item in work:
        item["inverse"] = eye - jnp.where(row // 2 == col // 2, item["pull"], 0.0)
        item["from_values"] = dot2(item["key_both"], item["value"])
    size = 2
    while size < CHUNK:
        joined = (row // (2 * size) == col // (2 * size)) & (row // size != col // size)
        halves = []
        for item in work:
            inverse = split(item["inverse"])
            between = split(jnp.where(joined, item["pull"], 0.0))
            halves.append((inverse, dot3(between, inverse)))
        for item, (inverse, half) in zip(work, halves):
            item["inverse"] = item["inverse"] - dot3(inverse, split(half))
        size *= 2
    key_row = lax.broadcasted_iota(jnp.int32, (HEAD, 2 * HEAD), 0)
    lane = lax.broadcasted_iota(jnp.int32, (HEAD, 2 * HEAD), 1)
    start = jnp.where(lane == key_row + HEAD, 1.0, 0.0)
    states = [start, start]
    for item in work:
        head = item["head"]
        state = states[head]
        from_start = dot3(item["query"], split(state)) + item["from_values"]
        pulled = dot3(split(item["inverse"]), split(from_start[:CHUNK]))
        pulled_parts = split(pulled)
        out_ref[pl.ds(item["chunk"] * CHUNK, CHUNK), pl.ds(head * 2 * HEAD, 2 * HEAD)] = (
            from_start[CHUNK:] - dot3(item["corr_read"], pulled_parts)
        )
        key_tail = tuple(t[:CHUNK] for t in item["tail"])
        corr_tail = tuple(t[CHUNK:] for t in item["tail"])
        states[head] = (
            item["keep"] * state
            + dot2(key_tail, item["value"], TN)
            + dot3(corr_tail, pulled_parts, TN)
        )
    for head in range(2):
        state_ref[pl.ds(head * HEAD, HEAD), :] = states[head].astype(jnp.bfloat16)


def read_kernel(place_ref, read_ref, maps_ref, gate_ref, gain_ref, out_ref):
    def one(step, carried):
        following = []
        for head in range(2):
            both = maps_ref[step, pl.ds(head * HEAD, HEAD), :]
            parts = split(carried[head])
            step_map = both[:, HEAD:]
            following.append(
                both[:, :HEAD].astype(jnp.float32)
                + dot(step_map, parts[0], NN)
                + dot(step_map, parts[1], NN)
            )
        return tuple(following)

    zero = jnp.zeros((HEAD, HEAD), jnp.float32)
    incoming = lax.fori_loop(0, place_ref[0], one, (zero, zero))
    scaled = []
    for head in range(2):
        both = read_ref[:, pl.ds(head * 2 * HEAD, 2 * HEAD)]
        state_read = both[:, :HEAD] + dot3(split(both[:, HEAD:]), split(incoming[head]))
        centred = state_read - jnp.mean(state_read, axis=1, keepdims=True)
        variance = jnp.mean(centred * centred, axis=1, keepdims=True)
        scaled.append(centred * lax.rsqrt(variance + EPS_GROUP))
    gated = (
        jnp.concatenate(scaled, axis=1)
        * gain_ref[...]
        * sigmoid(gate_ref[...].astype(jnp.float32))
    )
    out_ref[...] = gated.astype(jnp.bfloat16)


def time_mix(
    receptance, key_vectors, value_vectors, decay_logits, rate_logits, gate_logits, group_gain
):
    tokens_here, channels = receptance.shape
    pairs = channels // (2 * HEAD)
    wide = pl.BlockSpec((tokens_here, 2 * HEAD), lambda i: (0, i))
    double = pl.BlockSpec((tokens_here, 4 * HEAD), lambda i: (0, i))
    reads, states = pl.pallas_call(
        mix_kernel,
        grid=(pairs,),
        in_specs=[wide] * 5,
        out_specs=[double, pl.BlockSpec((2 * HEAD, 2 * HEAD), lambda i: (i, 0))],
        out_shape=[
            jax.ShapeDtypeStruct((tokens_here, 2 * channels), jnp.float32),
            jax.ShapeDtypeStruct((channels, 2 * HEAD), jnp.bfloat16),
        ],
        name="mix",
    )(receptance, key_vectors, value_vectors, decay_logits, rate_logits)
    maps = lax.all_gather(states, "sp")
    place = lax.axis_index("sp").astype(jnp.int32).reshape(1)
    return pl.pallas_call(
        read_kernel,
        grid=(pairs,),
        in_specs=[
            pl.BlockSpec(memory_space=pltpu.SMEM),
            double,
            pl.BlockSpec((maps.shape[0], 2 * HEAD, 2 * HEAD), lambda i: (0, i, 0)),
            wide,
            pl.BlockSpec((1, 2 * HEAD), lambda i: (0, i)),
        ],
        out_specs=wide,
        out_shape=jax.ShapeDtypeStruct((tokens_here, channels), jnp.bfloat16),
        name="read",
    )(place, reads, maps, gate_logits, group_gain.reshape(1, channels))


def exchange(x, axis, shape, source, target, collective_id, name):
    def kernel(x_ref, out_ref, stage, send_sem, recv_sem, local_sem):
        n = lax.axis_size(axis)
        me = lax.axis_index(axis)
        peers = [lax.rem(me + step, n) for step in range(1, n)]
        barrier = pltpu.get_barrier_semaphore()
        for peer in peers:
            pl.semaphore_signal(
                barrier, inc=1, device_id={axis: peer}, device_id_type=pl.DeviceIdType.MESH
            )
        pl.semaphore_wait(barrier, n - 1)
        copies = []
        for step, peer in enumerate(peers):
            copy = pltpu.make_async_remote_copy(
                src_ref=source(x_ref, peer),
                dst_ref=target(out_ref, me),
                send_sem=send_sem.at[step],
                recv_sem=recv_sem.at[step],
                device_id={axis: peer},
                device_id_type=pl.DeviceIdType.MESH,
            )
            copy.start()
            copies.append(copy)
        own = pltpu.make_async_copy(source(x_ref, me), stage, local_sem)
        own.start()
        own.wait()
        own = pltpu.make_async_copy(stage, target(out_ref, me), local_sem)
        own.start()
        own.wait()
        for copy in copies:
            copy.wait()

    n = lax.axis_size(axis)
    return pl.pallas_call(
        kernel,
        in_specs=[pl.BlockSpec(memory_space=pl.ANY)],
        out_specs=pl.BlockSpec(memory_space=pl.ANY),
        out_shape=jax.ShapeDtypeStruct(shape, x.dtype),
        scratch_shapes=[
            pltpu.VMEM(x.shape[-2:], x.dtype),
            pltpu.SemaphoreType.DMA((n - 1,)),
            pltpu.SemaphoreType.DMA((n - 1,)),
            pltpu.SemaphoreType.DMA,
        ],
        compiler_params=pltpu.CompilerParams(collective_id=collective_id, has_side_effects=True),
        name=name,
    )(x)


def gather_columns(x, axis, collective_id):
    rows, columns = x.shape
    return exchange(
        x,
        axis,
        (rows, lax.axis_size(axis) * columns),
        lambda ref, peer: ref,
        lambda ref, me: ref.at[:, pl.ds(pl.multiple_of(me * columns, columns), columns)],
        collective_id,
        "gather_columns",
    )


def gather_rows(x, axis, collective_id):
    rows, columns = x.shape
    return exchange(
        x,
        axis,
        (lax.axis_size(axis) * rows, columns),
        lambda ref, peer: ref,
        lambda ref, me: ref.at[pl.ds(pl.multiple_of(me * rows, rows), rows), :],
        collective_id,
        "gather_rows",
    )


def swap_blocks(x, axis, collective_id):
    return exchange(
        x, axis, x.shape, lambda ref, peer: ref.at[peer], lambda ref, me: ref.at[me],
        collective_id, "swap_blocks",
    )


def local(
    receptance,
    key_vectors,
    value_vectors,
    decay_logits,
    rate_logits,
    gate_logits,
    group_gain,
    residual,
    mixer_out,
    norm_gain,
    expert_ids,
    route_weight,
    expert_gate,
    expert_up,
    expert_down,
):
    mixed_rows = time_mix(
        receptance, key_vectors, value_vectors, decay_logits, rate_logits, gate_logits, group_gain
    )
    tokens_here, features = residual.shape
    projected = jnp.dot(
        gather_columns(mixed_rows, "tp", 0),
        mixer_out,
        preferred_element_type=jnp.float32,
    )
    midway = (residual.astype(jnp.float32) + projected).astype(jnp.bfloat16)
    midway_f = midway.astype(jnp.float32)
    squares = lax.psum(jnp.sum(midway_f * midway_f, axis=1), "tp")
    inv_rms = lax.rsqrt(squares / D + EPS_NORM)
    normed = (midway_f * norm_gain[None, :] * inv_rms[:, None]).astype(jnp.bfloat16)
    routes = expert_ids.shape[1]
    experts_all = lax.axis_size("sp") * expert_gate.shape[0]
    capacity = 2 * tokens_here * routes // experts_all
    flat_ids = expert_ids.reshape(-1)
    onehot = (flat_ids[:, None] == jnp.arange(experts_all, dtype=jnp.int32)[None, :]).astype(
        jnp.int32
    )
    earlier_count = jnp.sum((jnp.cumsum(onehot, axis=0) - onehot) * onehot, axis=1)
    slot_of = flat_ids * capacity + earlier_count
    owner_token = jnp.arange(tokens_here * routes, dtype=jnp.int32) // routes
    slot_table = (
        jnp.full((experts_all * capacity,), tokens_here, jnp.int32).at[slot_of].set(owner_token)
    )
    padded = jnp.concatenate([normed, jnp.zeros((1, features), jnp.bfloat16)], axis=0)
    outgoing = padded[slot_table].reshape(experts_all, capacity, features)
    arrived = swap_blocks(outgoing, "sp", 2)
    arrived_rows = arrived.reshape(-1, features)
    paired = jnp.concatenate([expert_gate[0], expert_up[0]], axis=1)
    gate_up = lax.psum_scatter(
        jnp.dot(arrived_rows, paired, preferred_element_type=jnp.float32).astype(jnp.bfloat16),
        "tp",
        scatter_dimension=0,
        tiled=True,
    ).astype(jnp.float32)
    half_width = paired.shape[1] // 2
    hidden = (jax.nn.silu(gate_up[:, :half_width]) * gate_up[:, half_width:]).astype(jnp.bfloat16)
    expert_res = jnp.dot(
        gather_rows(hidden, "tp", 1),
        expert_down[0],
        preferred_element_type=jnp.float32,
    )
    returned = swap_blocks(
        expert_res.astype(jnp.bfloat16).reshape(-1, capacity, features), "sp", 3
    )
    picked = (
        returned.reshape(-1, features)[slot_of]
        .astype(jnp.float32)
        .reshape(tokens_here, routes, features)
    )
    routed_sum = jnp.sum(picked * route_weight[:, :, None], axis=1)
    return (midway_f + routed_sum).astype(jnp.bfloat16)


def solution(mesh):
    placed = (
        P("sp", "tp"),
        P("sp", "tp"),
        P("sp", "tp"),
        P("sp", "tp"),
        P("sp", "tp"),
        P("sp", "tp"),
        P("tp"),
        P("sp", "tp"),
        P(None, "tp"),
        P("tp"),
        P("sp", None),
        P("sp", None),
        P("sp", "tp", None),
        P("sp", "tp", None),
        P("sp", None, "tp"),
    )
    return jax.shard_map(
        local, mesh=mesh, in_specs=placed, out_specs=P("sp", "tp"), check_vma=False
    )
```

profile of v0, /device:TPU:9, one launch (start us, length us, event | category | flops | bytes accessed | tf_op | source)
XLA Modules:
  0.0 356.7 jit_solution(15476126800678838836)
XLA Ops:
  6.5 0.0 copy-start
  6.5 0.0 copy-start.3
  6.5 0.0 all-gather.3.cloned.1.call-start
  6.5 42.8 %mix.1 = (f32[256,2048]{1,0:T(8,128)}, bf16[1024,128]{1,0:T(8,128)(2,1)}) custom-call(bf16[256,1024]{1,0:T(8,128)(2,1)} %r_ref.1, bf16[256,1024]{1,0:T(8,128)(2,1)} %k_ref.1, bf16[256,1024]{1,0:T(8,128)(2,1)} %v_ref.1, bf16[256,1024]{1,0:T(8,128)(2,1)} %d_ref.1, bf16[256,1024]{1,0:T(8,128)(2,1)} %a_ref.1), custom_call_target="tpu_custom_call" | custom-call | tf_op jit(solution)/shard_map/mix/pallas_call | solution.py:189
  49.3 0.0 all-gather.3.cloned.1.call-update
  49.3 0.0 reduce-scatter.2.cloned.1.call-start
  49.4 0.0 copy-done.3
  49.4 0.1 copy.18
  49.5 0.1 eq.29
  49.7 0.1 eq.25
  49.8 1.1 reduce-window.6
  51.0 0.2 slice_reduce_fusion
  51.2 0.1 copy.17
  51.4 0.1 mul.60
  51.6 0.1 fusion.19
  51.6 2.4 scatter_custom_fusion
  54.1 26.1 %all-gather.3.cloned.1.call-done = bf16[8192,128]{1,0:T(8,128)(2,1)} async-done(((bf16[1024,128]{1,0:T(8,128)(2,1)}), bf16[8192,128]{1,0:T(8,128)(2,1)}) %all-gather.3.cloned.1.call-update) | async-done | bytes 2097168 | tf_op jit(solution)/shard_map/all_gather | solution.py:200
  80.2 11.8 %read.1.x_ref = bf16[256,1024]{1,0:T(8,128)(2,1)} custom-call(s32[1]{0:T(128)} %bitcast.place_ref, f32[256,2048]{1,0:T(8,128)} %get-tuple-element.7.read_ref, bf16[8,1024,128]{2,1,0:T(8,128)(2,1)} %bitcast.30, bf16[256,1024]{1,0:T(8,128)(2,1)} %gate_ref.1, f32[1,1024]{1,0:T(1,128)} %bitcast.36), custom_call_target="tpu_custom_call" | custom-call | tf_op jit(solution)/shard_map/read/pallas_call | solution.py:202
  92.0 0.0 copy-start.6
  92.0 25.4 %gather_columns.1 = bf16[256,4096]{1,0:T(8,128)(2,1)} custom-call(bf16[256,1024]{1,0:T(8,128)(2,1)} %read.1.x_ref), custom_call_target="tpu_custom_call" | custom-call | tf_op jit(solution)/shard_map/gather_columns/pallas_call | solution.py:251
  117.4 0.0 copy-done.6
  117.4 0.0 copy-start.4
  117.4 6.5 %fusion.15 = (f32[256]{0:T(256)S(1)}, bf16[256,1024]{1,0:T(8,128)(2,1)S(1)}) fusion(bf16[256,4096]{1,0:T(8,128)(2,1)} %gather_columns.1, bf16[4096,1024]{1,0:T(8,128)(2,1)} %param.23, bf16[256,1024]{1,0:T(8,128)(2,1)S(1)} %copy-done.6), kind=kOutput, calls=%fused_computation.19 | convolution fusion | flops 2149056256 | bytes 11535360 | tf_op jit(solution)/shard_map/dot_general | solution.py:321
  123.9 0.0 copy-start.1
  123.9 7.8 %psum.7 = f32[256]{0:T(256)S(1)} all-reduce(f32[256]{0:T(256)S(1)} %get-tuple-element.9), channel_id=1, replica_groups=mesh['sp'=8,'tp'=4] {'tp'}, use_global_device_ids=true, to_apply=%region_1.0 | all-reduce | flops 256 | bytes 2048 | tf_op jit(solution)/shard_map/psum | solution.py:328
  131.7 0.0 copy-done.1
  131.7 0.0 copy-done.4
  131.7 0.2 fusion.14
  131.9 5.4 %gather_fusion = bf16[1024,1024]{1,0:T(8,128)(2,1)} fusion(bf16[257,1024]{1,0:T(8,128)(2,1)S(1)} %concatenate.6, s32[1024]{0:T(1024)S(1)} %fusion.21), kind=kCustom, calls=%fused_computation | custom fusion | bytes 4198400 | tf_op jit(solution)/shard_map/gather | solution.py:345
  137.3 55.5 %swap_blocks.2 = bf16[8,128,1024]{2,1,0:T(8,128)(2,1)} custom-call(bf16[8,128,1024]{2,1,0:T(8,128)(2,1)} %bitcast.29), custom_call_target="tpu_custom_call" | custom-call | tf_op jit(solution)/shard_map/swap_blocks/pallas_call | solution.py:251
  192.8 9.3 %fusion.4 = bf16[1024,2048]{1,0:T(8,128)(2,1)} fusion(bf16[1024,1024]{1,0:T(8,128)(2,1)} %bitcast.31, bf16[1024,1024]{1,0:T(8,128)(2,1)} %bitcast.37, bf16[1024,1024]{1,0:T(8,128)(2,1)} %bitcast.38), kind=kOutput, calls=%fused_computation.7 | convolution fusion | flops 4305453056 | bytes 10485760 | tf_op jit(solution)/shard_map/dot_general | solution.py:350
  202.1 0.0 copy-start.5
  202.1 0.0 reduce-scatter.2.cloned.1.call-update
  202.2 0.7 copy-done.5
  202.8 0.1 copy.20
  203.0 51.3 %reduce-scatter.2.cloned.1.call-done = bf16[256,2048]{1,0:T(8,128)(2,1)} async-done(((bf16[1024,2048]{1,0:T(8,128)(2,1)}), bf16[256,2048]{1,0:T(8,128)(2,1)}) %reduce-scatter.2.cloned.1.call-update) | async-done | bytes 1048592 | tf_op jit(solution)/shard_map/reduce_scatter | solution.py:349
  254.2 1.5 convert_element_type.48
  255.7 1.1 fusion.17.x_ref
  256.8 26.4 %gather_rows.1 = bf16[1024,1024]{1,0:T(8,128)(2,1)} custom-call(bf16[256,1024]{1,0:T(8,128)(2,1)} %fusion.17.x_ref), custom_call_target="tpu_custom_call" | custom-call | tf_op jit(solution)/shard_map/gather_rows/pallas_call | solution.py:251
  283.2 0.0 copy-done
  283.2 5.3 %fusion.9 = bf16[1024,1024]{1,0:T(8,128)(2,1)} fusion(bf16[1024,1024]{1,0:T(8,128)(2,1)} %gather_rows.1, bf16[1,1024,1024]{2,1,0:T(8,128)(2,1)S(1)} %copy-done), kind=kOutput, calls=%fused_computation.11 | convolution fusion | flops 2148532224 | bytes 6291456 | tf_op jit(solution)/shard_map/dot_general | solution.py:357
  288.5 49.2 %swap_blocks.3 = bf16[8,128,1024]{2,1,0:T(8,128)(2,1)} custom-call(bf16[8,128,1024]{2,1,0:T(8,128)(2,1)} %bitcast.32), custom_call_target="tpu_custom_call" | custom-call | tf_op jit(solution)/shard_map/swap_blocks/pallas_call | solution.py:251
  337.6 4.6 %gather_fusion.1 = bf16[512,1024]{1,0:T(8,128)(2,1)S(1)} fusion(bf16[1024,1024]{1,0:T(8,128)(2,1)} %bitcast.28, s32[1024]{0:T(1024)S(1)} %pad_clamp_fusion), kind=kCustom, calls=%fused_computation.1 | custom fusion | bytes 2099200 | tf_op jit(solution)/shard_map/gather | solution.py:366
  342.2 2.4 reshape.78
  344.6 0.0 copy-start.2
  344.6 4.3 %multiply_reduce_fusion = f32[256,1024]{1,0:T(8,128)S(1)} fusion(f32[256,2,1024]{2,1,0:T(2,128)} %reshape.78, f32[256,2]{1,0:T(8,128)S(1)} %copy.20), kind=kLoop, calls=%fused_computation.10 | loop fusion | flops 786432 | bytes 3147776 | tf_op jit(solution)/shard_map/reduce_sum | solution.py:370
  349.0 0.0 copy-done.2
  349.0 0.9 fusion.16
  (10 shorter events, 0.1 us)
Async XLA Ops:
  6.5 276.6 %copy-start = (bf16[1,1024,1024]{2,1,0:T(8,128)(2,1)S(1)}, bf16[1,1024,1024]{2,1,0:T(8,128)(2,1)}, u32[]{:S(2)}) copy-start(bf16[1,1024,1024]{2,1,0:T(8,128)(2,1)} %param.29) | copy-start | bytes 6291460
  6.5 42.8 %copy-start.3 = (s32[256,2]{0,1:T(2,128)S(1)}, s32[256,2]{0,1:T(2,128)}, u32[]{:S(2)}) copy-start(s32[256,2]{0,1:T(2,128)} %param.25) | copy-start | bytes 6148
  6.5 73.7 %all-gather.3.cloned.1.call-start = ((), (), s32[]{:S(2)}) async-start(), calls=%async_computation.2 | async-start | bytes 2359296 | tf_op jit(solution)/shard_map/all_gather | solution.py:200
  49.3 204.9 %reduce-scatter.2.cloned.1.call-start = ((), (), s32[]{:S(2)}) async-start(), calls=%async_computation.1 | async-start | bytes 5242880 | tf_op jit(solution)/shard_map/reduce_scatter | solution.py:349
  92.0 25.4 %copy-start.6 = (bf16[256,1024]{1,0:T(8,128)(2,1)S(1)}, bf16[256,1024]{1,0:T(8,128)(2,1)}, u32[]{:S(2)}) copy-start(bf16[256,1024]{1,0:T(8,128)(2,1)} %param.22) | copy-start | bytes 1572868
  117.4 14.3 %copy-start.4 = (f32[1024]{0:T(1024)S(1)}, f32[1024]{0:T(1024)}, u32[]{:S(2)}) copy-start(f32[1024]{0:T(1024)} %param.24) | copy-start | bytes 12292
  123.9 7.8 %copy-start.1 = (bf16[256,1024]{1,0:T(8,128)(2,1)}, bf16[256,1024]{1,0:T(8,128)(2,1)S(1)}, u32[]{:S(2)}) copy-start(bf16[256,1024]{1,0:T(8,128)(2,1)S(1)} %get-tuple-element.10) | copy-start | bytes 1572868
  202.1 0.7 copy-start.5
  344.6 4.3 %copy-start.2 = (bf16[256,1024]{1,0:T(8,128)(2,1)S(1)}, bf16[256,1024]{1,0:T(8,128)(2,1)}, u32[]{:S(2)}) copy-start(bf16[256,1024]{1,0:T(8,128)(2,1)} %copy-done.1) | copy-start | bytes 1572868
Sparse Core Ops, SparseCore 0:
  49.4 30.7 all-gather.2
  202.3 51.9 reduce-scatter.1
where the time goes:
time: 357 us
  Pallas kernels  211 us (59%)
  waiting for transfers between devices  77.4 us (22%)
  matrix products  21 us (6%)
  local copies, waits for them, and re-layouts  16.5 us (5%)
  between operations  13.6 us (4%)
  other arithmetic  9.32 us (3%)
  blocking collectives  7.79 us (2%)
    pallas_call x4, Pallas kernels, exchange(): pl.pallas_call(kernel, in_specs=[pl.BlockSpec(memory_space=pl.ANY)], out_...  156 us
    reduce_scatter x1, waiting for transfers between devices, local(): lax.psum_scatter(jnp.dot(arrived_rows, paired, preferred_element_type=jnp...  51.3 us
    pallas_call x1, Pallas kernels, time_mix(): pl.pallas_call(mix_kernel, grid=(pairs,), in_specs=[wide] * 5, out_specs=...  42.8 us
    all_gather x1, waiting for transfers between devices, time_mix(): maps = lax.all_gather(states, 'sp')  26.1 us
    pallas_call x1, Pallas kernels, time_mix(): pl.pallas_call(read_kernel, grid=(pairs,), in_specs=[pl.BlockSpec(memory_...  11.8 us
    dot_general x1, matrix products, local(): jnp.dot(arrived_rows, paired, preferred_element_type=jnp.float32)  9.29 us
    psum x1, blocking collectives, local(): squares = lax.psum(jnp.sum(midway_f * midway_f, axis=1), 'tp')  7.79 us
  transfers between devices with their start and end apart: 2, of which 2 were waited for; matrix products, arithmetic and copies ran while one was open for 1% of the time, Pallas kernels for 0%

commit v1 on v0

--- a/solution.py
+++ b/solution.py
@@ -297,6 +297,408 @@
     )
 
 
+MESH = pl.DeviceIdType.MESH
+GROUPS = 4
+
+
+def expert_kernel(
+    normed_ref,
+    midway_ref,
+    ids_ref,
+    weight_ref,
+    gate_hbm,
+    up_hbm,
+    down_hbm,
+    out_ref,
+    gate_w,
+    up_w,
+    down_w,
+    select,
+    outgoing,
+    aux_out,
+    aux_in,
+    rows_in,
+    part_a,
+    part_b,
+    first_a,
+    first_b,
+    pass_a,
+    pass_b,
+    second_a,
+    second_b,
+    hidden_a,
+    hidden_b,
+    own_res,
+    pair_out,
+    pair_in,
+    back_out,
+    back_in,
+    load_sem,
+    disp_send,
+    disp_recv,
+    aux_send,
+    aux_recv,
+    fwd_send,
+    fwd_recv,
+    tp_send,
+    tp_recv,
+    pair_send,
+    pair_recv,
+    back_send,
+    back_recv,
+):
+    tokens = normed_ref.shape[0]
+    slots = outgoing.shape[1]
+    quarter = slots // 4
+    half = slots // 2
+    width = hidden_a.shape[2]
+    peers = GROUPS
+    blocks = 2 * peers
+    sp = lax.axis_index("sp")
+    tp = lax.axis_index("tp")
+    z, core = sp // 2, sp % 2
+    y, x = tp // 2, tp % 2
+    x_peer = y * 2 + (1 - x)
+    y_peer = (1 - y) * 2 + x
+
+    def chip(turn):
+        step = (2 * turn - turn // 2) % 4
+        return 2 * ((z // 2 + step // 2) % 2) + (z % 2 + step % 2) % 2
+
+    loads = [
+        pltpu.make_async_copy(source.at[0], target, load_sem.at[i])
+        for i, (source, target) in enumerate(((gate_hbm, gate_w), (up_hbm, up_w), (down_hbm, down_w)))
+    ]
+    for load in loads:
+        load.start()
+
+    partner = {"sp": z * 2 + (1 - core)}
+    barrier = pltpu.get_barrier_semaphore()
+    friends = [partner, {"tp": x_peer}, {"tp": y_peer}]
+    friends += [{"sp": chip(turn) * 2 + core} for turn in range(1, peers)]
+    for friend in friends:
+        pl.semaphore_signal(barrier, inc=1, device_id=friend, device_id_type=MESH)
+
+    def remote(source, target, send, recv, device):
+        return pltpu.make_async_remote_copy(
+            src_ref=source, dst_ref=target, send_sem=send, recv_sem=recv,
+            device_id=device, device_id_type=MESH,
+        )
+
+    def dispatch(turn):
+        return remote(
+            outgoing.at[turn], rows_in.at[2 * turn], disp_send.at[turn], disp_recv.at[turn],
+            {"sp": chip(turn) * 2 + core},
+        )
+
+    def dispatch_aux(turn):
+        return remote(
+            aux_out.at[turn], aux_in.at[turn], aux_send.at[turn], aux_recv.at[turn],
+            {"sp": chip(turn) * 2 + core},
+        )
+
+    def forward(turn):
+        return remote(
+            rows_in.at[2 * turn], rows_in.at[2 * turn + 1], fwd_send.at[turn], fwd_recv.at[turn], partner
+        )
+
+    def over_tp(kind, k, source, target, device):
+        return remote(source, target, tp_send.at[kind, k], tp_recv.at[kind, k], {"tp": device})
+
+    def rows(start, size):
+        return pl.ds(pl.multiple_of(start, quarter), size)
+
+    def sum_first(k):
+        return (
+            over_tp(0, k, part_a.at[k, rows(half * (1 - x), half)], first_a.at[k], x_peer),
+            over_tp(1, k, part_b.at[k, rows(half * (1 - y), half)], first_b.at[k], y_peer),
+        )
+
+    def sum_second(k):
+        return (
+            over_tp(2, k, pass_a.at[k], second_a.at[k], y_peer),
+            over_tp(3, k, pass_b.at[k], second_b.at[k], x_peer),
+        )
+
+    def spread_first(k):
+        own_a = hidden_a.at[k, rows(half * x + quarter * y, quarter)]
+        own_b = hidden_b.at[k, rows(half * y + quarter * x, quarter)]
+        return (over_tp(4, k, own_a, own_a, y_peer), over_tp(5, k, own_b, own_b, x_peer))
+
+    def spread_second(k):
+        own_a = hidden_a.at[k, rows(half * x, half)]
+        own_b = hidden_b.at[k, rows(half * y, half)]
+        return (over_tp(6, k, own_a, own_a, x_peer), over_tp(7, k, own_b, own_b, y_peer))
+
+    def pair(turn):
+        return remote(pair_out.at[turn], pair_in.at[turn], pair_send.at[turn], pair_recv.at[turn], partner)
+
+    def give_back(turn):
+        return remote(
+            back_out.at[turn], back_in.at[turn], back_send.at[turn], back_recv.at[turn],
+            {"sp": chip(turn) * 2 + core},
+        )
+
+    ids = ids_ref[...]
+    weights = weight_ref[...]
+    lane = lax.broadcasted_iota(jnp.int32, (tokens, 128), 1)
+    slot_lane = lax.broadcasted_iota(jnp.int32, (tokens, slots), 1).astype(jnp.float32)
+    earlier = jnp.where(
+        lax.broadcasted_iota(jnp.int32, (tokens, tokens), 1)
+        < lax.broadcasted_iota(jnp.int32, (tokens, tokens), 0),
+        1.0,
+        0.0,
+    ).astype(jnp.bfloat16)
+    group_of = [chip(turn) for turn in range(peers)]
+    member = [
+        jnp.logical_and(ids[:, :1] >= 2 * group, ids[:, :1] < 2 * group + 2) for group in group_of
+    ]
+    members = jnp.zeros((tokens, 128), jnp.float32)
+    for turn in range(peers):
+        members = jnp.where(jnp.logical_and(lane == turn, member[turn]), 1.0, members)
+    ranks = dot(earlier, members.astype(jnp.bfloat16), NN)
+    normed = normed_ref[...]
+    pl.semaphore_wait(barrier, len(friends))
+    for turn in range(peers):
+        chosen = jnp.where(
+            jnp.logical_and(slot_lane == ranks[:, turn : turn + 1], member[turn]), 1.0, 0.0
+        ).astype(jnp.bfloat16)
+        select[turn] = chosen
+        picked = dot(chosen, normed, TN).astype(jnp.bfloat16)
+        if turn == 0:
+            rows_in[0] = picked
+            forward(0).start()
+        else:
+            outgoing[turn] = picked
+            dispatch(turn).start()
+        parts = jnp.zeros((tokens, 128), jnp.float32)
+        for expert in range(2):
+            name = 2 * group_of[turn] + expert
+            value = jnp.where(ids[:, :1] == name, weights[:, :1], 0.0) + jnp.where(
+                ids[:, 1:2] == name, weights[:, 1:2], 0.0
+            )
+            for piece in range(3):
+                term = value.astype(jnp.bfloat16).astype(jnp.float32)
+                parts = jnp.where(lane == 3 * expert + piece, term, parts)
+                value = value - term
+        by_slot = dot(parts.astype(jnp.bfloat16), chosen, TN)
+        weight_rows = jnp.concatenate(
+            [
+                by_slot[0:1] + by_slot[1:2] + by_slot[2:3],
+                by_slot[3:4] + by_slot[4:5] + by_slot[5:6],
+                jnp.zeros((6, slots), jnp.float32),
+            ],
+            axis=0,
+        )
+        if turn == 0:
+            aux_in[0] = weight_rows
+        else:
+            aux_out[turn] = weight_rows
+            dispatch_aux(turn).start()
+    for load in loads:
+        load.wait()
+
+    def step(t, carry):
+        @pl.when(t < blocks)
+        def _():
+            k = t
+            turn = k // 2
+
+            @pl.when(jnp.logical_and(k % 2 == 0, k > 0))
+            def _():
+                dispatch(turn).wait_recv()
+                forward(turn).start()
+
+            @pl.when(k % 2 == 1)
+            def _():
+                forward(turn).wait_recv()
+
+            block = rows_in[k]
+            for part, columns in ((part_a, pl.ds(0, width)), (part_b, pl.ds(width, width))):
+                part[k, :, :width] = dot(block, gate_w[:, columns], NN).astype(jnp.bfloat16)
+                part[k, :, width:] = dot(block, up_w[:, columns], NN).astype(jnp.bfloat16)
+            for copy in sum_first(k):
+                copy.start()
+
+        @pl.when(jnp.logical_and(t >= 1, t < blocks + 1))
+        def _():
+            k = t - 1
+            copies = sum_first(k)
+            nexts = sum_second(k)
+            copies[0].wait_recv()
+            pass_a[k] = (
+                part_a[k, rows(half * x + quarter * (1 - y), quarter)].astype(jnp.float32)
+                + first_a[k, rows(quarter * (1 - y), quarter)].astype(jnp.float32)
+            ).astype(jnp.bfloat16)
+            nexts[0].start()
+            copies[1].wait_recv()
+            pass_b[k] = (
+                part_b[k, rows(half * y + quarter * (1 - x), quarter)].astype(jnp.float32)
+                + first_b[k, rows(quarter * (1 - x), quarter)].astype(jnp.float32)
+            ).astype(jnp.bfloat16)
+            nexts[1].start()
+
+        @pl.when(jnp.logical_and(t >= 2, t < blocks + 2))
+        def _():
+            k = t - 2
+            copies = sum_second(k)
+            nexts = spread_first(k)
+            for i, (part, first, second, hidden, major, minor) in enumerate(
+                (
+                    (part_a, first_a, second_a, hidden_a, x, y),
+                    (part_b, first_b, second_b, hidden_b, y, x),
+                )
+            ):
+                copies[i].wait_recv()
+                mine = rows(half * major + quarter * minor, quarter)
+                total = (
+                    part[k, mine].astype(jnp.float32)
+                    + first[k, rows(quarter * minor, quarter)].astype(jnp.float32)
+                    + second[k].astype(jnp.float32)
+                )
+                gate, up = total[:, :width], total[:, width:]
+                hidden[k, mine] = (gate * sigmoid(gate) * up).astype(jnp.bfloat16)
+                nexts[i].start()
+
+        @pl.when(jnp.logical_and(t >= 3, t < blocks + 3))
+        def _():
+            k = t - 3
+            for copy, follow in zip(spread_first(k), spread_second(k)):
+                copy.wait_recv()
+                follow.start()
+
+        @pl.when(jnp.logical_and(t >= 4, t < blocks + 4))
+        def _():
+            k = t - 4
+            turn = k // 2
+            for copy in spread_second(k):
+                copy.wait_recv()
+            result = dot(hidden_a[k], down_w[:width, :], NN) + dot(hidden_b[k], down_w[width:, :], NN)
+
+            @pl.when(k % 2 == 0)
+            def _():
+                own_res[turn] = result
+
+            @pl.when(k % 2 == 1)
+            def _():
+                pair_out[turn] = result.astype(jnp.bfloat16)
+                pair(turn).start()
+
+        @pl.when(jnp.logical_and(t >= 6, t % 2 == 0))
+        def _():
+            turn = (t - 6) // 2
+
+            @pl.when(turn > 0)
+            def _():
+                dispatch_aux(turn).wait_recv()
+
+            pair(turn).wait_recv()
+            columns = jnp.concatenate([aux_in[turn]] * (128 // 8), axis=0).T
+            low, high = columns[:, 0:1], columns[:, 1:2]
+            mine = jnp.where(core == 0, low, high)
+            other = jnp.where(core == 0, high, low)
+            both = (own_res[turn] * mine + pair_in[turn].astype(jnp.float32) * other).astype(
+                jnp.bfloat16
+            )
+
+            @pl.when(turn == 0)
+            def _():
+                back_in[0] = both
+
+            @pl.when(turn > 0)
+            def _():
+                back_out[turn] = both
+                give_back(turn).start()
+
+        return carry
+
+    lax.fori_loop(0, blocks + 5, step, 0)
+    total = midway_ref[...].astype(jnp.float32)
+    for turn in range(peers):
+        if turn > 0:
+            give_back(turn).wait_recv()
+        total = total + dot(select[turn], back_in[turn], NN)
+    out_ref[...] = total.astype(jnp.bfloat16)
+
+    for turn in range(peers):
+        forward(turn).wait_send()
+        pair(turn).wait_send()
+        if turn > 0:
+            dispatch(turn).wait_send()
+            dispatch_aux(turn).wait_send()
+            give_back(turn).wait_send()
+
+    def drain(k, carry):
+        for copies in (sum_first(k), sum_second(k), spread_first(k), spread_second(k)):
+            for copy in copies:
+                copy.wait_send()
+        return carry
+
+    lax.fori_loop(0, blocks, drain, 0)
+
+
+def routed_experts(normed, midway, expert_ids, route_weight, expert_gate, expert_up, expert_down):
+    tokens, features = normed.shape
+    hidden = expert_gate.shape[2]
+    half = hidden // 2
+    slots = tokens // 2
+    quarter = slots // 4
+    peers = GROUPS
+    blocks = 2 * peers
+    bf = jnp.bfloat16
+    whole = pl.BlockSpec(memory_space=pltpu.VMEM)
+    far = pl.BlockSpec(memory_space=pl.ANY)
+    dma = pltpu.SemaphoreType.DMA
+    return pl.pallas_call(
+        expert_kernel,
+        in_specs=[whole] * 4 + [far] * 3,
+        out_specs=whole,
+        out_shape=jax.ShapeDtypeStruct((tokens, features), bf),
+        scratch_shapes=[
+            pltpu.VMEM((features, hidden), bf),
+            pltpu.VMEM((features, hidden), bf),
+            pltpu.VMEM((hidden, features), bf),
+            pltpu.VMEM((peers, tokens, slots), bf),
+            pltpu.VMEM((peers, slots, features), bf),
+            pltpu.VMEM((peers, 8, slots), jnp.float32),
+            pltpu.VMEM((peers, 8, slots), jnp.float32),
+            pltpu.VMEM((blocks, slots, features), bf),
+            pltpu.VMEM((blocks, slots, hidden), bf),
+            pltpu.VMEM((blocks, slots, hidden), bf),
+            pltpu.VMEM((blocks, slots // 2, hidden), bf),
+            pltpu.VMEM((blocks, slots // 2, hidden), bf),
+            pltpu.VMEM((blocks, quarter, hidden), bf),
+            pltpu.VMEM((blocks, quarter, hidden), bf),
+            pltpu.VMEM((blocks, quarter, hidden), bf),
+            pltpu.VMEM((blocks, quarter, hidden), bf),
+            pltpu.VMEM((blocks, slots, half), bf),
+            pltpu.VMEM((blocks, slots, half), bf),
+            pltpu.VMEM((peers, slots, features), jnp.float32),
+            pltpu.VMEM((peers, slots, features), bf),
+            pltpu.VMEM((peers, slots, features), bf),
+            pltpu.VMEM((peers, slots, features), bf),
+            pltpu.VMEM((peers, slots, features), bf),
+            dma((3,)),
+            dma((peers,)),
+            dma((peers,)),
+            dma((peers,)),
+            dma((peers,)),
+            dma((peers,)),
+            dma((peers,)),
+            dma((8, blocks)),
+            dma((8, blocks)),
+            dma((peers,)),
+            dma((peers,)),
+            dma((peers,)),
+            dma((peers,)),
+        ],
+        compiler_params=pltpu.CompilerParams(
+            collective_id=4, has_side_effects=True, vmem_limit_bytes=52 * 1024 * 1024
+        ),
+        name="experts",
+    )(normed, midway, expert_ids, route_weight, expert_gate, expert_up, expert_down)
+
+
 def local(
     receptance,
     key_vectors,
@@ -329,6 +731,11 @@
     inv_rms = lax.rsqrt(squares / D + EPS_NORM)
     normed = (midway_f * norm_gain[None, :] * inv_rms[:, None]).astype(jnp.bfloat16)
     routes = expert_ids.shape[1]
+    paired_cores = lax.axis_size("sp") == 2 * GROUPS and lax.axis_size("tp") == 4
+    if paired_cores and expert_gate.shape[0] == 1:
+        return routed_experts(
+            normed, midway, expert_ids, route_weight, expert_gate, expert_up, expert_down
+        )
     experts_all = lax.axis_size("sp") * expert_gate.shape[0]
     capacity = 2 * tokens_here * routes // experts_all
     flat_ids = expert_ids.reshape(-1)

time: 357 us -> 228 us (0.64)
  the two profiles are of different devices: /device:TPU:9 before, /device:TPU:0 now
where the time goes in v1:
time: 228 us
  Pallas kernels  165 us (72%)
  waiting for transfers between devices  31.7 us (14%)
  between operations  13.5 us (6%)
  blocking collectives  9.53 us (4%)
  matrix products  6.47 us (3%)
    pallas_call x1, Pallas kernels, routed_experts(): pl.pallas_call(expert_kernel, in_specs=[whole] * 4 + [far] * 3, out_specs...  87.3 us
    pallas_call x1, Pallas kernels, time_mix(): pl.pallas_call(mix_kernel, grid=(pairs,), in_specs=[wide] * 5, out_specs=...  42.6 us
    all_gather x1, waiting for transfers between devices, time_mix(): maps = lax.all_gather(states, 'sp')  31.7 us
    pallas_call x1, Pallas kernels, exchange(): pl.pallas_call(kernel, in_specs=[pl.BlockSpec(memory_space=pl.ANY)], out_...  27.3 us
    psum x1, blocking collectives, local(): squares = lax.psum(jnp.sum(midway_f * midway_f, axis=1), 'tp')  9.53 us
    pallas_call x1, Pallas kernels, time_mix(): pl.pallas_call(read_kernel, grid=(pairs,), in_specs=[pl.BlockSpec(memory_...  8.01 us
    dot_general x1, matrix products, local(): jnp.dot(gather_columns(mixed_rows, 'tp', 0), mixer_out, preferred_element...  6.47 us
  transfers between devices with their start and end apart: 1, of which 1 were waited for; matrix products, arithmetic and copies ran while one was open for 0% of the time, Pallas kernels for 0%

profile of v1, /device:TPU:0, one launch (start us, length us, event | category | flops | bytes accessed | tf_op | source)
XLA Modules:
  0.0 227.7 jit_solution(9780397766775233110)
XLA Ops:
  6.5 0.0 copy-start.1
  6.5 0.0 copy-start.2
  6.5 0.0 all-gather.3.cloned.1.call-start
  6.5 42.6 %mix.1 = (f32[256,2048]{1,0:T(8,128)}, bf16[1024,128]{1,0:T(8,128)(2,1)}) custom-call(bf16[256,1024]{1,0:T(8,128)(2,1)} %r_ref.1, bf16[256,1024]{1,0:T(8,128)(2,1)} %k_ref.1, bf16[256,1024]{1,0:T(8,128)(2,1)} %v_ref.1, bf16[256,1024]{1,0:T(8,128)(2,1)} %d_ref.1, bf16[256,1024]{1,0:T(8,128)(2,1)} %a_ref.1), custom_call_target="tpu_custom_call" | custom-call | tf_op jit(solution)/shard_map/mix/pallas_call | solution.py:189
  49.2 0.0 all-gather.3.cloned.1.call-update
  49.2 0.0 copy-done.1
  49.2 0.1 copy.16.ids_ref
  49.3 0.0 copy-done.2
  49.4 0.1 copy.17.weight_ref
  49.5 31.7 %all-gather.3.cloned.1.call-done = bf16[8192,128]{1,0:T(8,128)(2,1)} async-done(((bf16[1024,128]{1,0:T(8,128)(2,1)}), bf16[8192,128]{1,0:T(8,128)(2,1)}) %all-gather.3.cloned.1.call-update) | async-done | bytes 2097168 | tf_op jit(solution)/shard_map/all_gather | solution.py:200
  81.2 8.0 %read.1.x_ref = bf16[256,1024]{1,0:T(8,128)(2,1)} custom-call(s32[1]{0:T(128)} %bitcast.place_ref, f32[256,2048]{1,0:T(8,128)} %get-tuple-element.7.read_ref, bf16[8,1024,128]{2,1,0:T(8,128)(2,1)} %bitcast.5, bf16[256,1024]{1,0:T(8,128)(2,1)} %gate_ref.1, f32[1,1024]{1,0:T(1,128)} %bitcast.6), custom_call_target="tpu_custom_call" | custom-call | tf_op jit(solution)/shard_map/read/pallas_call | solution.py:202
  89.2 0.0 copy-start.3
  89.2 27.3 %gather_columns.1 = bf16[256,4096]{1,0:T(8,128)(2,1)} custom-call(bf16[256,1024]{1,0:T(8,128)(2,1)} %read.1.x_ref), custom_call_target="tpu_custom_call" | custom-call | tf_op jit(solution)/shard_map/gather_columns/pallas_call | solution.py:251
  116.5 0.0 copy-done.3
  116.5 0.0 copy-start
  116.6 6.5 %fusion.3 = (f32[256]{0:T(256)S(1)}, bf16[256,1024]{1,0:T(8,128)(2,1)S(1)}) fusion(bf16[256,4096]{1,0:T(8,128)(2,1)} %gather_columns.1, bf16[4096,1024]{1,0:T(8,128)(2,1)} %param.23, bf16[256,1024]{1,0:T(8,128)(2,1)S(1)} %copy-done.3), kind=kOutput, calls=%fused_computation.6 | convolution fusion | flops 2149056256 | bytes 11535360 | tf_op jit(solution)/shard_map/dot_general | solution.py:723
  123.0 9.5 %psum.7 = f32[256]{0:T(256)S(1)} all-reduce(f32[256]{0:T(256)S(1)} %get-tuple-element.9), channel_id=1, replica_groups=mesh['sp'=8,'tp'=4] {'tp'}, use_global_device_ids=true, to_apply=%region_1.0 | all-reduce | flops 256 | bytes 2048 | tf_op jit(solution)/shard_map/psum | solution.py:730
  132.6 0.0 copy-done
  132.6 0.2 fusion.2.normed_ref
  132.8 87.3 %experts.1 = bf16[256,1024]{1,0:T(8,128)(2,1)S(1)} custom-call(bf16[256,1024]{1,0:T(8,128)(2,1)S(1)} %fusion.2.normed_ref, bf16[256,1024]{1,0:T(8,128)(2,1)S(1)} %get-tuple-element.10.midway_ref, s32[256,2]{1,0:T(8,128)S(1)} %copy.16.ids_ref, f32[256,2]{1,0:T(8,128)S(1)} %copy.17.weight_ref, bf16[1,1024,1024]{2,1,0:T(8,128)(2,1)} %gate_hbm.1, ...), custom_call_target="tpu_custom_call" | custom-call | tf_op jit(solution)/shard_map/experts/pallas_call | solution.py:652
  220.0 0.8 copy.19
  (1 shorter events, 0.0 us)
Async XLA Ops:
  6.5 42.7 %copy-start.1 = (s32[256,2]{0,1:T(2,128)S(1)}, s32[256,2]{0,1:T(2,128)}, u32[]{:S(2)}) copy-start(s32[256,2]{0,1:T(2,128)} %param.25) | copy-start | bytes 6148
  6.5 42.8 %copy-start.2 = (f32[256,2]{0,1:T(2,128)S(1)}, f32[256,2]{0,1:T(2,128)}, u32[]{:S(2)}) copy-start(f32[256,2]{0,1:T(2,128)} %param.26) | copy-start | bytes 6148
  6.5 74.7 %all-gather.3.cloned.1.call-start = ((), (), s32[]{:S(2)}) async-start(), calls=%async_computation | async-start | bytes 2359296 | tf_op jit(solution)/shard_map/all_gather | solution.py:200
  89.2 27.3 %copy-start.3 = (bf16[256,1024]{1,0:T(8,128)(2,1)S(1)}, bf16[256,1024]{1,0:T(8,128)(2,1)}, u32[]{:S(2)}) copy-start(bf16[256,1024]{1,0:T(8,128)(2,1)} %param.22) | copy-start | bytes 1572868
  116.5 16.0 %copy-start = (f32[1024]{0:T(1024)S(1)}, f32[1024]{0:T(1024)}, u32[]{:S(2)}) copy-start(f32[1024]{0:T(1024)} %param.24) | copy-start | bytes 12292
Sparse Core Ops, SparseCore 0:
  49.3 31.8 all-gather.2

commit v2 on v1

--- a/solution.py
+++ b/solution.py
@@ -299,6 +299,453 @@
 
 MESH = pl.DeviceIdType.MESH
 GROUPS = 4
+
+
+def pack_left(a):
+    hi, lo = split(a)
+    return jnp.concatenate([hi, lo], axis=1)
+
+
+def pack_right(b):
+    both = jnp.concatenate(split(b), axis=1)
+    return jnp.concatenate([both, both], axis=0)
+
+
+def dot_packed(left, right):
+    out = dot(left, right, NN)
+    n = out.shape[1] // 2
+    return out[:, :n] + out[:, n:]
+
+
+def three(a, axis, second):
+    hi, lo = split(a)
+    return jnp.concatenate([hi, hi, lo] if second else [hi, lo, hi], axis=axis)
+
+
+def mix_heads(recept_in, key_in, values_in, decay_in, rate_in, write_read, write_state):
+    tokens, width = recept_in.shape
+    chunks = tokens // CHUNK
+    pairs = width // (2 * HEAD)
+    row = lax.broadcasted_iota(jnp.int32, (CHUNK, CHUNK), 0)
+    col = lax.broadcasted_iota(jnp.int32, (CHUNK, CHUNK), 1)
+    strict = col < row
+    causal = col <= row
+    eye = jnp.where(col == row, 1.0, 0.0)
+    ones_lower = jnp.where(causal, 1.0, 0.0).astype(jnp.bfloat16)
+    ones_twice = jnp.concatenate([ones_lower, ones_lower], axis=1)
+    low = lax.broadcasted_iota(jnp.int32, (CHUNK, 2 * HEAD), 1) < HEAD
+    nothing = jnp.zeros((CHUNK, 2 * HEAD), jnp.bfloat16)
+
+    work = []
+    for chunk in range(chunks):
+        rows = slice(chunk * CHUNK, (chunk + 1) * CHUNK)
+        for pair in range(pairs):
+            lanes = slice(pair * 2 * HEAD, (pair + 1) * 2 * HEAD)
+            recept = recept_in[rows, lanes].astype(jnp.float32)
+            keyvec = key_in[rows, lanes].astype(jnp.float32)
+            values = values_in[rows, lanes]
+            logdec = -EXP_HALF * sigmoid(decay_in[rows, lanes].astype(jnp.float32))
+            first, second = split(logdec)
+            third = (logdec - first.astype(jnp.float32) - second.astype(jnp.float32)).astype(
+                jnp.bfloat16
+            )
+            cum_in = dot_packed(
+                ones_twice,
+                jnp.concatenate(
+                    [
+                        jnp.concatenate([first, third], axis=1),
+                        jnp.concatenate([second, nothing], axis=1),
+                    ],
+                    axis=0,
+                ),
+            )
+            cum_end = cum_in[CHUNK - 1 :, :]
+            squares = keyvec * keyvec
+            norms = jnp.where(
+                low,
+                jnp.sum(squares[:, :HEAD], axis=1, keepdims=True),
+                jnp.sum(squares[:, HEAD:], axis=1, keepdims=True),
+            )
+            unit_key = keyvec * lax.rsqrt(1.0 + norms)
+            correction = unit_key * sigmoid(rate_in[rows, lanes].astype(jnp.float32))
+            growth = jnp.exp(-cum_in)
+            tail = jnp.exp(cum_end - cum_in)
+            r_scaled = recept * jnp.exp(cum_in)
+            u_scaled = unit_key * jnp.exp(cum_in - logdec)
+            queries = jnp.concatenate([u_scaled, r_scaled], axis=0)
+            sources = jnp.concatenate([keyvec * growth, correction * growth], axis=0)
+            tails = jnp.concatenate([(keyvec * tail).T, -(correction * tail).T], axis=1)
+            tail_hi, tail_lo = split(tails)
+            keep = jnp.broadcast_to(jnp.exp(cum_end), (2 * HEAD, 2 * HEAD)).T
+            for head in range(2):
+                part = slice(head * HEAD, (head + 1) * HEAD)
+                query = three(queries[:, part], 1, False)
+                scores = dot(query, three(sources[:, part], 1, True), NT)
+                value = jnp.concatenate(
+                    [values[:, part], jnp.zeros((CHUNK, HEAD), jnp.bfloat16)], axis=1
+                )
+                work.append(
+                    dict(
+                        head=2 * pair + head,
+                        chunk=chunk,
+                        query=query,
+                        tail=jnp.concatenate([tail_hi[part, :], tail_lo[part, :]], axis=0),
+                        keep=keep[part, :],
+                        value=value,
+                        key_both=pack_left(
+                            jnp.concatenate(
+                                [
+                                    jnp.where(strict, scores[:CHUNK, :CHUNK], 0.0),
+                                    jnp.where(causal, scores[CHUNK:, :CHUNK], 0.0),
+                                ],
+                                axis=0,
+                            )
+                        ),
+                        pull=jnp.where(strict, scores[:CHUNK, CHUNK:], 0.0),
+                        corr_read=pack_left(jnp.where(causal, scores[CHUNK:, CHUNK:], 0.0)),
+                    )
+                )
+    for item in work:
+        item["inverse"] = eye - jnp.where(row // 2 == col // 2, item["pull"], 0.0)
+        value = item["value"]
+        item["from_values"] = dot(
+            item["key_both"], jnp.concatenate([value, value], axis=0), NN
+        )
+    size = 2
+    while size < CHUNK:
+        joined = (row // (2 * size) == col // (2 * size)) & (row // size != col // size)
+        halves = []
+        for item in work:
+            between = pack_left(jnp.where(joined, item["pull"], 0.0))
+            halves.append(dot_packed(between, pack_right(item["inverse"])))
+        for item, half in zip(work, halves):
+            item["inverse"] = item["inverse"] - dot_packed(
+                pack_left(item["inverse"]), pack_right(half)
+            )
+        size *= 2
+    key_row = lax.broadcasted_iota(jnp.int32, (HEAD, 2 * HEAD), 0)
+    lane = lax.broadcasted_iota(jnp.int32, (HEAD, 2 * HEAD), 1)
+    start = jnp.where(lane == key_row + HEAD, 1.0, 0.0)
+    states = [start] * (2 * pairs)
+    for chunk in range(chunks):
+        items = [item for item in work if item["chunk"] == chunk]
+        froms = [
+            dot(item["query"], three(states[item["head"]], 0, True), NN) + item["from_values"]
+            for item in items
+        ]
+        pulls = [
+            dot_packed(pack_left(item["inverse"]), pack_right(value[:CHUNK]))
+            for item, value in zip(items, froms)
+        ]
+        for item, value, pulled in zip(items, froms, pulls):
+            head = item["head"]
+            write_read(
+                chunk, head, value[CHUNK:] - dot_packed(item["corr_read"], pack_right(pulled))
+            )
+            hi, lo = split(pulled)
+            right = jnp.concatenate(
+                [
+                    jnp.concatenate([item["value"], hi], axis=0),
+                    jnp.concatenate([nothing, lo], axis=0),
+                ],
+                axis=1,
+            )
+            out = dot(item["tail"], right, NN)
+            states[head] = (
+                item["keep"] * states[head]
+                + (out[:HEAD, : 2 * HEAD] + out[HEAD:, : 2 * HEAD])
+                + out[:HEAD, 2 * HEAD :]
+            )
+    for head in range(2 * pairs):
+        write_state(head, states[head].astype(jnp.bfloat16))
+
+
+def mixer_kernel(
+    r_ref,
+    k_ref,
+    v_ref,
+    d_ref,
+    a_ref,
+    gate_ref,
+    gain_ref,
+    residual_ref,
+    norm_ref,
+    mixer_hbm,
+    normed_ref,
+    midway_ref,
+    mixer_w,
+    reads,
+    maps_own,
+    maps_in,
+    joint,
+    carry_out,
+    carry_in,
+    gathered,
+    acc,
+    sums,
+    load_sem,
+    swap_send,
+    swap_recv,
+    chain_send,
+    chain_recv,
+    gather_send,
+    gather_recv,
+    sum_send,
+    sum_recv,
+):
+    tokens, features = residual_ref.shape
+    steps, _, wide = reads.shape
+    width = wide // 2
+    heads = width // HEAD
+    tps = lax.axis_size("tp")
+    chips = lax.axis_size("sp") // 2
+    sp = lax.axis_index("sp")
+    tp = lax.axis_index("tp")
+    z, core = sp // 2, sp % 2
+    partner = {"sp": z * 2 + (1 - core)}
+    peers = [{"tp": (tp + shift) % tps} for shift in range(1, tps)]
+
+    def load(step, block):
+        return pltpu.make_async_copy(
+            mixer_hbm.at[pl.ds(pl.multiple_of(block * steps * width + step * width, width), width), :],
+            mixer_w.at[step, pl.ds(block * width, width), :],
+            load_sem.at[step, block],
+        )
+
+    def load_all(step, carry):
+        for block in range(tps):
+            load(step, block).start()
+        return carry
+
+    lax.fori_loop(0, steps, load_all, 0)
+
+    barrier = pltpu.get_barrier_semaphore()
+    friends = [partner] + peers
+    friends += [{"sp": ((z + shift) % chips) * 2 + core} for shift in (1, chips - 1)]
+    for friend in friends:
+        pl.semaphore_signal(barrier, inc=1, device_id=friend, device_id_type=MESH)
+    acc[...] = residual_ref[...].astype(jnp.float32)
+    pl.semaphore_wait(barrier, len(friends))
+
+    def remote(source, target, send, recv, device):
+        return pltpu.make_async_remote_copy(
+            src_ref=source, dst_ref=target, send_sem=send, recv_sem=recv,
+            device_id=device, device_id_type=MESH,
+        )
+
+    def swap(j):
+        return remote(maps_own.at[j], maps_in.at[j], swap_send.at[j], swap_recv.at[j], partner)
+
+    def chain(j):
+        return remote(
+            carry_out.at[j], carry_in.at[j], chain_send.at[j], chain_recv.at[j],
+            {"sp": ((z + 1) % chips) * 2 + core},
+        )
+
+    def columns():
+        return pl.ds(pl.multiple_of(tp * width, width), width)
+
+    def gather(j):
+        own = gathered.at[j, :, columns()]
+        return [
+            remote(own, own, gather_send.at[i, j], gather_recv.at[i, j], peer)
+            for i, peer in enumerate(peers)
+        ]
+
+    def mix(i):
+        lanes = pl.ds(pl.multiple_of(i * width, width), width)
+
+        def write_read(chunk, head, value):
+            reads[i, pl.ds(chunk * CHUNK, CHUNK), pl.ds(head * 2 * HEAD, 2 * HEAD)] = value
+
+        def write_state(head, value):
+            maps_own[i, pl.ds(head * HEAD, HEAD), :] = value
+
+        mix_heads(
+            r_ref[:, lanes], k_ref[:, lanes], v_ref[:, lanes], d_ref[:, lanes], a_ref[:, lanes],
+            write_read, write_state,
+        )
+        swap(i).start()
+
+    half_lane = lax.broadcasted_iota(jnp.int32, (HEAD, 2 * HEAD), 1) < HEAD
+
+    def join(j):
+        swap(j).wait_recv()
+        for head in range(heads):
+            part = pl.ds(head * HEAD, HEAD)
+            own, other = maps_own[j, part, :], maps_in[j, part, :]
+            first = jnp.where(core == 0, own, other)
+            second = jnp.where(core == 0, other, own)
+            both = dot(second[:, HEAD:], first, NN)
+            joint[j, part, :] = both + jnp.where(half_lane, second.astype(jnp.float32), 0.0)
+
+    def follow(j):
+        @pl.when(z > 0)
+        def _():
+            chain(j).wait_recv()
+
+        @pl.when(z == 0)
+        def _():
+            carry_in[j] = jnp.zeros((HEAD, width), jnp.float32)
+
+        carried = [carry_in[j, :, pl.ds(head * HEAD, HEAD)] for head in range(heads)]
+        carried_parts = [split(value) for value in carried]
+        following = []
+        for head in range(heads):
+            both = joint[j, pl.ds(head * HEAD, HEAD), :]
+            following.append(both[:, :HEAD] + dot3(split(both[:, HEAD:]), carried_parts[head]))
+        carry_out[j] = jnp.concatenate(following, axis=1)
+
+        @pl.when(z < chips - 1)
+        def _():
+            chain(j).start()
+
+        mine = []
+        for head in range(heads):
+            other = maps_in[j, pl.ds(head * HEAD, HEAD), :]
+            passed = other[:, :HEAD].astype(jnp.float32) + (
+                dot(other[:, HEAD:], carried_parts[head][0], NN)
+                + dot(other[:, HEAD:], carried_parts[head][1], NN)
+            )
+            mine.append(jnp.where(core == 0, carried[head], passed))
+        lanes = pl.ds(pl.multiple_of(j * width, width), width)
+        blank = jnp.zeros((HEAD, 2 * HEAD), jnp.bfloat16)
+        scaled = []
+        for head in range(heads):
+            both = reads[j, :, pl.ds(head * 2 * HEAD, 2 * HEAD)]
+            state = jnp.concatenate([blank, jnp.concatenate(split(mine[head]), axis=1)], axis=0)
+            out = dot(pack_left(both), jnp.concatenate([state, state], axis=0), NN)
+            state_read = both[:, :HEAD] + (out[:, :HEAD] + out[:, HEAD:])
+            centred = state_read - jnp.mean(state_read, axis=1, keepdims=True)
+            variance = jnp.mean(centred * centred, axis=1, keepdims=True)
+            scaled.append(centred * lax.rsqrt(variance + EPS_GROUP))
+        gated = (
+            jnp.concatenate(scaled, axis=1)
+            * gain_ref[:, lanes]
+            * sigmoid(gate_ref[:, lanes].astype(jnp.float32))
+        )
+        gathered[j, :, columns()] = gated.astype(jnp.bfloat16)
+        for copy in gather(j):
+            copy.start()
+
+    def project(j):
+        for block in range(tps):
+            load(j, block).wait()
+        for copy in gather(j):
+            copy.wait_recv()
+        acc[...] += dot(gathered[j], mixer_w[j], NN)
+
+    def within(j):
+        return jnp.logical_and(j >= 0, j < steps)
+
+    def step(t, carry):
+        @pl.when(within(t - 2 - z))
+        def _():
+            follow(t - 2 - z)
+
+        @pl.when(within(t - 4 - z))
+        def _():
+            project(t - 4 - z)
+
+        @pl.when(within(t))
+        def _():
+            mix(t)
+
+        @pl.when(within(t - 1))
+        def _():
+            join(t - 1)
+
+        return carry
+
+    lax.fori_loop(0, steps + chips + 3, step, 0)
+
+    midway = acc[...].astype(jnp.bfloat16)
+    midway_ref[...] = midway
+    midway_f = midway.astype(jnp.float32)
+    squares = jnp.sum(midway_f * midway_f, axis=1, keepdims=True)
+    sums[0] = jnp.broadcast_to(squares, (tokens, 128)).T[:8, :]
+    copies = [
+        remote(sums.at[0], sums.at[i + 1], sum_send.at[i], sum_recv.at[i], peer)
+        for i, peer in enumerate(peers)
+    ]
+    for copy in copies:
+        copy.start()
+    scaled = midway_f * norm_ref[...]
+    for copy in copies:
+        copy.wait_recv()
+    total = sums[0]
+    for i in range(1, tps):
+        total = total + sums[i]
+    total = jnp.concatenate([total] * (128 // 8), axis=0).T[:, :1]
+    normed_ref[...] = (scaled * lax.rsqrt(total / D + EPS_NORM)).astype(jnp.bfloat16)
+
+    for copy in copies:
+        copy.wait_send()
+
+    def drain(j, carry):
+        swap(j).wait_send()
+
+        @pl.when(z < chips - 1)
+        def _():
+            chain(j).wait_send()
+
+        for copy in gather(j):
+            copy.wait_send()
+        return carry
+
+    lax.fori_loop(0, steps, drain, 0)
+
+
+HEADS_PER_STEP = 2
+
+
+def mixed_tokens(
+    receptance, key_vectors, value_vectors, decay_logits, rate_logits, gate_logits, group_gain,
+    residual, mixer_out, norm_gain,
+):
+    tokens, channels = receptance.shape
+    features = residual.shape[1]
+    tps = lax.axis_size("tp")
+    width = HEADS_PER_STEP * HEAD
+    steps = channels // width
+    bf = jnp.bfloat16
+    f32 = jnp.float32
+    whole = pl.BlockSpec(memory_space=pltpu.VMEM)
+    dma = pltpu.SemaphoreType.DMA
+    return pl.pallas_call(
+        mixer_kernel,
+        in_specs=[whole] * 9 + [pl.BlockSpec(memory_space=pl.ANY)],
+        out_specs=[whole, whole],
+        out_shape=[jax.ShapeDtypeStruct((tokens, features), bf)] * 2,
+        scratch_shapes=[
+            pltpu.VMEM((steps, tps * width, features), bf),
+            pltpu.VMEM((steps, tokens, 2 * width), f32),
+            pltpu.VMEM((steps, width, 2 * HEAD), bf),
+            pltpu.VMEM((steps, width, 2 * HEAD), bf),
+            pltpu.VMEM((steps, width, 2 * HEAD), f32),
+            pltpu.VMEM((steps, HEAD, width), f32),
+            pltpu.VMEM((steps, HEAD, width), f32),
+            pltpu.VMEM((steps, tokens, tps * width), bf),
+            pltpu.VMEM((tokens, features), f32),
+            pltpu.VMEM((tps, 8, tokens), f32),
+            dma((steps, tps)),
+            dma((steps,)),
+            dma((steps,)),
+            dma((steps,)),
+            dma((steps,)),
+            dma((tps - 1, steps)),
+            dma((tps - 1, steps)),
+            dma((tps - 1,)),
+            dma((tps - 1,)),
+        ],
+        compiler_params=pltpu.CompilerParams(
+            collective_id=5, has_side_effects=True, vmem_limit_bytes=56 * 1024 * 1024
+        ),
+        name="mixer",
+    )(
+        receptance, key_vectors, value_vectors, decay_logits, rate_logits, gate_logits,
+        group_gain.reshape(1, channels), residual, norm_gain.reshape(1, features), mixer_out,
+    )
 
 
 def expert_kernel(
@@ -716,6 +1163,15 @@
     expert_up,
     expert_down,
 ):
+    paired_cores = lax.axis_size("sp") == 2 * GROUPS and lax.axis_size("tp") == 4
+    if paired_cores and expert_gate.shape[0] == 1:
+        normed, midway = mixed_tokens(
+            receptance, key_vectors, value_vectors, decay_logits, rate_logits, gate_logits,
+            group_gain, residual, mixer_out, norm_gain,
+        )
+        return routed_experts(
+            normed, midway, expert_ids, route_weight, expert_gate, expert_up, expert_down
+        )
     mixed_rows = time_mix(
         receptance, key_vectors, value_vectors, decay_logits, rate_logits, gate_logits, group_gain
     )
@@ -731,11 +1187,6 @@
     inv_rms = lax.rsqrt(squares / D + EPS_NORM)
     normed = (midway_f * norm_gain[None, :] * inv_rms[:, None]).astype(jnp.bfloat16)
     routes = expert_ids.shape[1]
-    paired_cores = lax.axis_size("sp") == 2 * GROUPS and lax.axis_size("tp") == 4
-    if paired_cores and expert_gate.shape[0] == 1:
-        return routed_experts(
-            normed, midway, expert_ids, route_weight, expert_gate, expert_up, expert_down
-        )
     experts_all = lax.axis_size("sp") * expert_gate.shape[0]
     capacity = 2 * tokens_here * routes // experts_all
     flat_ids = expert_ids.reshape(-1)

time: 228 us -> 160 us (0.70)
  waiting for transfers between devices: 31.7 us -> 0 us
  between operations: 13.5 us -> 0.04 us
  blocking collectives: 9.53 us -> 0 us
  Pallas kernels: 165 us -> 156 us
  matrix products: 6.47 us -> 0 us
  local copies, waits for them, and re-layouts: 1.08 us -> 4.49 us
    all_gather x1 -> x0, waiting for transfers between devices: 31.7 us -> none  [time_mix(): maps = lax.all_gather(states, 'sp')]
    pallas_call x3 -> x1, Pallas kernels: 77.9 us -> 67.6 us  [mixed_tokens(): pl.pallas_call(mixer_kernel, in_specs=[whole] * 9 + [pl.BlockSpec(memory_...]
    psum x1 -> x0, blocking collectives: 9.53 us -> none  [local(): squares = lax.psum(jnp.sum(midway_f * midway_f, axis=1), 'tp')]
    dot_general x1 -> x0, matrix products: 6.47 us -> none  [local(): jnp.dot(gather_columns(mixed_rows, 'tp', 0), mixer_out, preferred_element...]
    unnamed x11 -> x7, local copies, waits for them, and re-layouts: 1.08 us -> 4.49 us
  transfers between devices with their start and end apart: 1 -> 0, of which waited for: 1 -> 0; matrix products, arithmetic and copies ran while one was open for 0% -> 0% of each run, Pallas kernels for 0% -> 0%
where the time goes in v2:
time: 160 us
  Pallas kernels  156 us (98%)
  local copies, waits for them, and re-layouts  4.49 us (3%)
    pallas_call x1, Pallas kernels, routed_experts(): pl.pallas_call(expert_kernel, in_specs=[whole] * 4 + [far] * 3, out_specs...  88.1 us
    pallas_call x1, Pallas kernels, mixed_tokens(): pl.pallas_call(mixer_kernel, in_specs=[whole] * 9 + [pl.BlockSpec(memory_...  67.6 us
    unnamed x7, local copies, waits for them, and re-layouts  4.49 us

profile of v2, /device:TPU:0, one launch (start us, length us, event | category | flops | bytes accessed | tf_op | source)
XLA Modules:
  0.0 160.2 jit_solution(3550397574709062209)
XLA Ops:
  0.0 0.8 copy.16.ids_ref
  0.8 0.8 copy.17.weight_ref
  1.6 67.6 %mixer.1 = (bf16[256,1024]{1,0:T(8,128)(2,1)}, bf16[256,1024]{1,0:T(8,128)(2,1)}) custom-call(bf16[256,1024]{1,0:T(8,128)(2,1)} %r_ref.1, bf16[256,1024]{1,0:T(8,128)(2,1)} %k_ref.1, bf16[256,1024]{1,0:T(8,128)(2,1)} %v_ref.1, bf16[256,1024]{1,0:T(8,128)(2,1)} %d_ref.1, bf16[256,1024]{1,0:T(8,128)(2,1)} %a_ref.1, bf16[256,1024]{1,0:T(8,128)(2,1)} %gate_ref.1, ...), custom_call_target="tpu_custom_call" | custom-call | tf_op jit(solution)/shard_map/mixer/pallas_call | solution.py:715
  69.2 0.0 copy-start
  69.2 1.0 copy-done
  70.2 0.0 copy-start.1
  70.2 1.0 copy-done.1
  71.3 88.1 %experts.1 = bf16[256,1024]{1,0:T(8,128)(2,1)S(1)} custom-call(bf16[256,1024]{1,0:T(8,128)(2,1)S(1)} %copy-done, bf16[256,1024]{1,0:T(8,128)(2,1)S(1)} %copy-done.1, s32[256,2]{1,0:T(8,128)S(1)} %copy.16.ids_ref, f32[256,2]{1,0:T(8,128)S(1)} %copy.17.weight_ref, bf16[1,1024,1024]{2,1,0:T(8,128)(2,1)} %gate_hbm.1, bf16[1,1024,1024]{2,1,0:T(8,128)(2,1)} %up_hbm.1, ...), custom_call_target="tpu_custom_call" | custom-call | tf_op jit(solution)/shard_map/experts/pallas_call | solution.py:1099
  159.4 0.8 copy.19
Async XLA Ops:
  69.2 1.0 copy-start
  70.2 1.0 copy-start.1

commit v3 on v2

--- a/solution.py
+++ b/solution.py
@@ -320,6 +320,25 @@
 def three(a, axis, second):
     hi, lo = split(a)
     return jnp.concatenate([hi, hi, lo] if second else [hi, lo, hi], axis=axis)
+
+
+def lower_rows(a, size):
+    starts = range(size, a.shape[0], 2 * size)
+    return jnp.concatenate([a[at : at + size] for at in starts], axis=0)
+
+
+def join_rows(a, lower, size):
+    parts = []
+    for i, at in enumerate(range(0, a.shape[0], 2 * size)):
+        parts += [a[at : at + size], lower[i * size : (i + 1) * size]]
+    return jnp.concatenate(parts, axis=0)
+
+
+def spread_rows(lower, size):
+    parts = []
+    for at in range(0, lower.shape[0], size):
+        parts += [jnp.zeros((size, lower.shape[1]), lower.dtype), lower[at : at + size]]
+    return jnp.concatenate(parts, axis=0)
 
 
 def mix_heads(recept_in, key_in, values_in, decay_in, rate_in, write_read, write_state):
@@ -415,13 +434,23 @@
     while size < CHUNK:
         joined = (row // (2 * size) == col // (2 * size)) & (row // size != col // size)
         halves = []
-        for item in work:
-            between = pack_left(jnp.where(joined, item["pull"], 0.0))
-            halves.append(dot_packed(between, pack_right(item["inverse"])))
-        for item, half in zip(work, halves):
-            item["inverse"] = item["inverse"] - dot_packed(
-                pack_left(item["inverse"]), pack_right(half)
-            )
+        if size < 8:
+            for item in work:
+                between = pack_left(jnp.where(joined, item["pull"], 0.0))
+                halves.append(dot_packed(between, pack_right(item["inverse"])))
+            for item, half in zip(work, halves):
+                item["inverse"] = item["inverse"] - dot_packed(
+                    pack_left(item["inverse"]), pack_right(half)
+                )
+        else:
+            for item in work:
+                between = pack_left(lower_rows(jnp.where(joined, item["pull"], 0.0), size))
+                halves.append(dot_packed(between, pack_right(item["inverse"])))
+            for item, half in zip(work, halves):
+                inverse = item["inverse"]
+                below = lower_rows(inverse, size)
+                update = dot_packed(pack_left(below), pack_right(spread_rows(half, size)))
+                item["inverse"] = join_rows(inverse, below - update, size)
         size *= 2
     key_row = lax.broadcasted_iota(jnp.int32, (HEAD, 2 * HEAD), 0)
     lane = lax.broadcasted_iota(jnp.int32, (HEAD, 2 * HEAD), 1)
@@ -478,8 +507,10 @@
     maps_own,
     maps_in,
     joint,
+    joint_in,
     carry_out,
     carry_in,
+    carried,
     gathered,
     acc,
     sums,
@@ -488,6 +519,8 @@
     swap_recv,
     chain_send,
     chain_recv,
+    joint_send,
+    joint_recv,
     gather_send,
     gather_recv,
     sum_send,
@@ -503,7 +536,10 @@
     tp = lax.axis_index("tp")
     z, core = sp // 2, sp % 2
     partner = {"sp": z * 2 + (1 - core)}
-    peers = [{"tp": (tp + shift) % tps} for shift in range(1, tps)]
+    y, x = tp // 2, tp % 2
+    x_peer = y * 2 + (1 - x)
+    y_peer = (1 - y) * 2 + x
+    peers = [{"tp": x_peer}, {"tp": y_peer}, {"tp": (1 - y) * 2 + (1 - x)}]
 
     def load(step, block):
         return pltpu.make_async_copy(
@@ -521,7 +557,7 @@
 
     barrier = pltpu.get_barrier_semaphore()
     friends = [partner] + peers
-    friends += [{"sp": ((z + shift) % chips) * 2 + core} for shift in (1, chips - 1)]
+    friends += [{"sp": ((z + shift) % chips) * 2 + core} for shift in range(1, chips)]
     for friend in friends:
         pl.semaphore_signal(barrier, inc=1, device_id=friend, device_id_type=MESH)
     acc[...] = residual_ref[...].astype(jnp.float32)
@@ -536,20 +572,33 @@
     def swap(j):
         return remote(maps_own.at[j], maps_in.at[j], swap_send.at[j], swap_recv.at[j], partner)
 
-    def chain(j):
+    def chain(j, hop, target):
         return remote(
-            carry_out.at[j], carry_in.at[j], chain_send.at[j], chain_recv.at[j],
-            {"sp": ((z + 1) % chips) * 2 + core},
-        )
-
-    def columns():
-        return pl.ds(pl.multiple_of(tp * width, width), width)
+            carry_out.at[j], carry_in.at[j], chain_send.at[hop, j], chain_recv.at[j],
+            {"sp": target * 2 + core},
+        )
+
+    def hand_joint(j):
+        return remote(
+            joint.at[j], joint_in.at[j], joint_send.at[j], joint_recv.at[j],
+            {"sp": (chips - 1) * 2 + core},
+        )
+
+    def columns(owner):
+        return pl.ds(pl.multiple_of(owner * width, width), width)
 
     def gather(j):
-        own = gathered.at[j, :, columns()]
+        own = gathered.at[j, :, columns(tp)]
         return [
-            remote(own, own, gather_send.at[i, j], gather_recv.at[i, j], peer)
-            for i, peer in enumerate(peers)
+            remote(own, own, gather_send.at[i, j], gather_recv.at[i, j], peers[i]) for i in range(2)
+        ]
+
+    def relay(j):
+        low = gathered.at[j, pl.ds(0, tokens // 2), columns(x_peer)]
+        high = gathered.at[j, pl.ds(tokens // 2, tokens // 2), columns(y_peer)]
+        return [
+            remote(low, low, gather_send.at[2, j], gather_recv.at[2, j], peers[1]),
+            remote(high, high, gather_send.at[3, j], gather_recv.at[3, j], peers[0]),
         ]
 
     def mix(i):
@@ -579,59 +628,102 @@
             both = dot(second[:, HEAD:], first, NN)
             joint[j, part, :] = both + jnp.where(half_lane, second.astype(jnp.float32), 0.0)
 
-    def follow(j):
-        @pl.when(z > 0)
-        def _():
-            chain(j).wait_recv()
-
         @pl.when(z == 0)
         def _():
-            carry_in[j] = jnp.zeros((HEAD, width), jnp.float32)
-
-        carried = [carry_in[j, :, pl.ds(head * HEAD, HEAD)] for head in range(heads)]
-        carried_parts = [split(value) for value in carried]
+            carry_out[j] = jnp.concatenate(
+                [joint[j, pl.ds(head * HEAD, HEAD), :][:, :HEAD] for head in range(heads)], axis=1
+            ).astype(jnp.bfloat16)
+            carried[j] = jnp.zeros((HEAD, width), jnp.bfloat16)
+            chain(j, 0, 1).start()
+
+        @pl.when(z == 2)
+        def _():
+            hand_joint(j).start()
+
+    def advance(maps, j):
         following = []
         for head in range(heads):
-            both = joint[j, pl.ds(head * HEAD, HEAD), :]
-            following.append(both[:, :HEAD] + dot3(split(both[:, HEAD:]), carried_parts[head]))
-        carry_out[j] = jnp.concatenate(following, axis=1)
-
-        @pl.when(z < chips - 1)
-        def _():
-            chain(j).start()
-
-        mine = []
+            both = maps[j, pl.ds(head * HEAD, HEAD), :]
+            value = carry_in[j, :, pl.ds(head * HEAD, HEAD)]
+            following.append(both[:, :HEAD] + dot2(split(both[:, HEAD:]), value))
+        return jnp.concatenate(following, axis=1).astype(jnp.bfloat16)
+
+    def hop(j):
+        chain(j, 0, 1).wait_recv()
+        carried[j] = carry_in[j]
+        carry_out[j] = advance(joint, j)
+        chain(j, 0, 2).start()
+        chain(j, 1, 3).start()
+
+    def finish(j):
+        @pl.when(z >= 2)
+        def _():
+            chain(j, 0, 1).wait_recv()
+
+        @pl.when(z == 2)
+        def _():
+            carried[j] = carry_in[j]
+
+        @pl.when(z == 3)
+        def _():
+            hand_joint(j).wait_recv()
+            carried[j] = advance(joint_in, j)
+
+        nothing = jnp.zeros((HEAD, HEAD), jnp.bfloat16)
+        unit = jnp.where(
+            lax.broadcasted_iota(jnp.int32, (HEAD, HEAD), 0)
+            == lax.broadcasted_iota(jnp.int32, (HEAD, HEAD), 1),
+            1.0,
+            0.0,
+        ).astype(jnp.bfloat16)
+        state_parts = []
         for head in range(heads):
+            value = carried[j, :, pl.ds(head * HEAD, HEAD)]
             other = maps_in[j, pl.ds(head * HEAD, HEAD), :]
-            passed = other[:, :HEAD].astype(jnp.float32) + (
-                dot(other[:, HEAD:], carried_parts[head][0], NN)
-                + dot(other[:, HEAD:], carried_parts[head][1], NN)
+            passed = other[:, :HEAD].astype(jnp.float32) + dot(other[:, HEAD:], value, NN)
+            state_parts.append(split(jnp.where(core == 0, value.astype(jnp.float32), passed)))
+        head_of = [
+            lax.broadcasted_iota(jnp.int32, (4 * HEAD, 2 * HEAD), axis) // HEAD % 2
+            for axis in range(2)
+        ]
+        average = jnp.where(head_of[0] == head_of[1], 1.0 / HEAD, 0.0).astype(jnp.bfloat16)
+        for pair in range(heads // 2):
+            here = [reads[j, :, pl.ds((2 * pair + i) * 2 * HEAD, 2 * HEAD)] for i in range(2)]
+            hi, lo = split(jnp.concatenate(here, axis=1))
+            (first_hi, first_lo), (second_hi, second_lo) = state_parts[2 * pair : 2 * pair + 2]
+            wide_rows = [
+                [unit, nothing, nothing, nothing],
+                [first_hi, nothing, first_lo, nothing],
+                [nothing, unit, nothing, nothing],
+                [nothing, second_hi, nothing, second_lo],
+            ]
+            right = jnp.concatenate(
+                [jnp.concatenate(blocks, axis=1) for blocks in wide_rows], axis=0
             )
-            mine.append(jnp.where(core == 0, carried[head], passed))
-        lanes = pl.ds(pl.multiple_of(j * width, width), width)
-        blank = jnp.zeros((HEAD, 2 * HEAD), jnp.bfloat16)
-        scaled = []
-        for head in range(heads):
-            both = reads[j, :, pl.ds(head * 2 * HEAD, 2 * HEAD)]
-            state = jnp.concatenate([blank, jnp.concatenate(split(mine[head]), axis=1)], axis=0)
-            out = dot(pack_left(both), jnp.concatenate([state, state], axis=0), NN)
-            state_read = both[:, :HEAD] + (out[:, :HEAD] + out[:, HEAD:])
-            centred = state_read - jnp.mean(state_read, axis=1, keepdims=True)
-            variance = jnp.mean(centred * centred, axis=1, keepdims=True)
-            scaled.append(centred * lax.rsqrt(variance + EPS_GROUP))
-        gated = (
-            jnp.concatenate(scaled, axis=1)
-            * gain_ref[:, lanes]
-            * sigmoid(gate_ref[:, lanes].astype(jnp.float32))
-        )
-        gathered[j, :, columns()] = gated.astype(jnp.bfloat16)
+            state_read = dot_packed(hi, right) + dot(lo, right[:, : 2 * HEAD], NN)
+            centred = state_read - dot(pack_left(state_read), average, NN)
+            variance = dot(pack_left(centred * centred), average, NN)
+            lanes = pl.ds(pl.multiple_of(j * width + pair * 2 * HEAD, 2 * HEAD), 2 * HEAD)
+            gated = (
+                centred
+                * lax.rsqrt(variance + EPS_GROUP)
+                * gain_ref[:, lanes]
+                * sigmoid(gate_ref[:, lanes].astype(jnp.float32))
+            )
+            own_lanes = pl.ds(pl.multiple_of(tp * width + pair * 2 * HEAD, 2 * HEAD), 2 * HEAD)
+            gathered[j, :, own_lanes] = gated.astype(jnp.bfloat16)
         for copy in gather(j):
             copy.start()
+
+    def pass_on(j):
+        for copy, after in zip(gather(j), relay(j)):
+            copy.wait_recv()
+            after.start()
 
     def project(j):
         for block in range(tps):
             load(j, block).wait()
-        for copy in gather(j):
+        for copy in relay(j):
             copy.wait_recv()
         acc[...] += dot(gathered[j], mixer_w[j], NN)
 
@@ -639,13 +731,9 @@
         return jnp.logical_and(j >= 0, j < steps)
 
     def step(t, carry):
-        @pl.when(within(t - 2 - z))
-        def _():
-            follow(t - 2 - z)
-
-        @pl.when(within(t - 4 - z))
-        def _():
-            project(t - 4 - z)
+        @pl.when(jnp.logical_and(z == 1, within(t - 2)))
+        def _():
+            hop(t - 2)
 
         @pl.when(within(t))
         def _():
@@ -655,9 +743,25 @@
         def _():
             join(t - 1)
 
+        @pl.when(jnp.logical_and(z == 0, within(t - 1)))
+        def _():
+            finish(t - 1)
+
+        @pl.when(jnp.logical_and(z > 0, within(t - 2)))
+        def _():
+            finish(t - 2)
+
+        @pl.when(within(t - 3))
+        def _():
+            pass_on(t - 3)
+
+        @pl.when(within(t - 4))
+        def _():
+            project(t - 4)
+
         return carry
 
-    lax.fori_loop(0, steps + chips + 3, step, 0)
+    lax.fori_loop(0, steps + 4, step, 0)
 
     midway = acc[...].astype(jnp.bfloat16)
     midway_ref[...] = midway
@@ -685,18 +789,26 @@
     def drain(j, carry):
         swap(j).wait_send()
 
-        @pl.when(z < chips - 1)
-        def _():
-            chain(j).wait_send()
-
-        for copy in gather(j):
+        @pl.when(z < 2)
+        def _():
+            chain(j, 0, 1).wait_send()
+
+        @pl.when(z == 1)
+        def _():
+            chain(j, 1, 1).wait_send()
+
+        @pl.when(z == 2)
+        def _():
+            hand_joint(j).wait_send()
+
+        for copy in gather(j) + relay(j):
             copy.wait_send()
         return carry
 
     lax.fori_loop(0, steps, drain, 0)
 
 
-HEADS_PER_STEP = 2
+HEADS_PER_STEP = 4
 
 
 def mixed_tokens(
@@ -723,18 +835,22 @@
             pltpu.VMEM((steps, width, 2 * HEAD), bf),
             pltpu.VMEM((steps, width, 2 * HEAD), bf),
             pltpu.VMEM((steps, width, 2 * HEAD), f32),
-            pltpu.VMEM((steps, HEAD, width), f32),
-            pltpu.VMEM((steps, HEAD, width), f32),
+            pltpu.VMEM((steps, width, 2 * HEAD), f32),
+            pltpu.VMEM((steps, HEAD, width), bf),
+            pltpu.VMEM((steps, HEAD, width), bf),
+            pltpu.VMEM((steps, HEAD, width), bf),
             pltpu.VMEM((steps, tokens, tps * width), bf),
             pltpu.VMEM((tokens, features), f32),
             pltpu.VMEM((tps, 8, tokens), f32),
             dma((steps, tps)),
             dma((steps,)),
             dma((steps,)),
+            dma((2, steps)),
             dma((steps,)),
             dma((steps,)),
-            dma((tps - 1, steps)),
-            dma((tps - 1, steps)),
+            dma((steps,)),
+            dma((4, steps)),
+            dma((4, steps)),
             dma((tps - 1,)),
             dma((tps - 1,)),
         ],
@@ -748,20 +864,26 @@
     )
 
 
+LAG = 1
+
+
 def expert_kernel(
-    normed_ref,
-    midway_ref,
+    normed_hbm,
+    midway_hbm,
     ids_ref,
     weight_ref,
     gate_hbm,
     up_hbm,
     down_hbm,
     out_ref,
+    normed_ref,
+    midway_ref,
     gate_w,
     up_w,
     down_w,
     select,
     outgoing,
+    factors,
     aux_out,
     aux_in,
     rows_in,
@@ -795,12 +917,14 @@
     back_recv,
 ):
     tokens = normed_ref.shape[0]
-    slots = outgoing.shape[1]
-    quarter = slots // 4
-    half = slots // 2
+    size = outgoing.shape[1]
+    slots = 2 * size
+    quarter = size // 4
+    half = size // 2
     width = hidden_a.shape[2]
     peers = GROUPS
-    blocks = 2 * peers
+    units = 2 * peers
+    blocks = 2 * units
     sp = lax.axis_index("sp")
     tp = lax.axis_index("tp")
     z, core = sp // 2, sp % 2
@@ -809,13 +933,21 @@
     y_peer = (1 - y) * 2 + x
 
     def chip(turn):
-        step = (2 * turn - turn // 2) % 4
-        return 2 * ((z // 2 + step // 2) % 2) + (z % 2 + step % 2) % 2
+        return 2 * ((z // 2 + turn // 2) % 2) + (z % 2 + turn % 2) % 2
+
+    def turn_of(q):
+        return (q + 6) // 8 + (q + 5) // 8 + (q + 3) // 8 - 2 * ((q + 1) // 8)
+
+    def half_of(q):
+        return (q + 7) // 8 - (q + 6) // 8 + (q + 4) // 8 - (q + 3) // 8 + (q + 2) // 8
 
     loads = [
         pltpu.make_async_copy(source.at[0], target, load_sem.at[i])
         for i, (source, target) in enumerate(((gate_hbm, gate_w), (up_hbm, up_w), (down_hbm, down_w)))
     ]
+    load_rows = pltpu.make_async_copy(normed_hbm, normed_ref, load_sem.at[3])
+    load_rows.start()
+    loads.append(pltpu.make_async_copy(midway_hbm, midway_ref, load_sem.at[4]))
     for load in loads:
         load.start()
 
@@ -832,10 +964,10 @@
             device_id=device, device_id_type=MESH,
         )
 
-    def dispatch(turn):
+    def dispatch(q):
         return remote(
-            outgoing.at[turn], rows_in.at[2 * turn], disp_send.at[turn], disp_recv.at[turn],
-            {"sp": chip(turn) * 2 + core},
+            outgoing.at[q], rows_in.at[2 * q], disp_send.at[q], disp_recv.at[q],
+            {"sp": chip(turn_of(q)) * 2 + core},
         )
 
     def dispatch_aux(turn):
@@ -844,10 +976,8 @@
             {"sp": chip(turn) * 2 + core},
         )
 
-    def forward(turn):
-        return remote(
-            rows_in.at[2 * turn], rows_in.at[2 * turn + 1], fwd_send.at[turn], fwd_recv.at[turn], partner
-        )
+    def forward(q):
+        return remote(rows_in.at[2 * q], rows_in.at[2 * q + 1], fwd_send.at[q], fwd_recv.at[q], partner)
 
     def over_tp(kind, k, source, target, device):
         return remote(source, target, tp_send.at[kind, k], tp_recv.at[kind, k], {"tp": device})
@@ -877,17 +1007,29 @@
         own_b = hidden_b.at[k, rows(half * y, half)]
         return (over_tp(6, k, own_a, own_a, x_peer), over_tp(7, k, own_b, own_b, y_peer))
 
-    def pair(turn):
-        return remote(pair_out.at[turn], pair_in.at[turn], pair_send.at[turn], pair_recv.at[turn], partner)
-
-    def give_back(turn):
+    def pair(q):
+        return remote(pair_out.at[q], pair_in.at[q], pair_send.at[q], pair_recv.at[q], partner)
+
+    def back_rows(q):
+        return pl.ds(pl.multiple_of(turn_of(q) * slots + half_of(q) * size, size), size)
+
+    def give_back(q):
         return remote(
-            back_out.at[turn], back_in.at[turn], back_send.at[turn], back_recv.at[turn],
-            {"sp": chip(turn) * 2 + core},
-        )
-
-    ids = ids_ref[...]
-    weights = weight_ref[...]
+            back_out.at[q], back_in.at[back_rows(q), :], back_send.at[q], back_recv.at[q],
+            {"sp": chip(turn_of(q)) * 2 + core},
+        )
+
+    def as_columns(few_rows):
+        return jnp.concatenate([few_rows] * (slots // 8), axis=0).T
+
+    def few_rows():
+        few = jnp.concatenate(
+            [ids_ref[...].astype(jnp.float32), weight_ref[...], jnp.zeros((4, tokens), jnp.float32)],
+            axis=0,
+        )
+        return jnp.concatenate([few] * (128 // 8), axis=0).T
+
+    ids = few_rows()[:, :2].astype(jnp.int32)
     lane = lax.broadcasted_iota(jnp.int32, (tokens, 128), 1)
     slot_lane = lax.broadcasted_iota(jnp.int32, (tokens, slots), 1).astype(jnp.float32)
     earlier = jnp.where(
@@ -904,61 +1046,75 @@
     for turn in range(peers):
         members = jnp.where(jnp.logical_and(lane == turn, member[turn]), 1.0, members)
     ranks = dot(earlier, members.astype(jnp.bfloat16), NN)
+    load_rows.wait()
     normed = normed_ref[...]
     pl.semaphore_wait(barrier, len(friends))
     for turn in range(peers):
         chosen = jnp.where(
             jnp.logical_and(slot_lane == ranks[:, turn : turn + 1], member[turn]), 1.0, 0.0
         ).astype(jnp.bfloat16)
-        select[turn] = chosen
+        select[:, turn * slots : (turn + 1) * slots] = chosen
         picked = dot(chosen, normed, TN).astype(jnp.bfloat16)
-        if turn == 0:
-            rows_in[0] = picked
-            forward(0).start()
-        else:
-            outgoing[turn] = picked
-            dispatch(turn).start()
-        parts = jnp.zeros((tokens, 128), jnp.float32)
-        for expert in range(2):
-            name = 2 * group_of[turn] + expert
-            value = jnp.where(ids[:, :1] == name, weights[:, :1], 0.0) + jnp.where(
-                ids[:, 1:2] == name, weights[:, 1:2], 0.0
-            )
-            for piece in range(3):
-                term = value.astype(jnp.bfloat16).astype(jnp.float32)
-                parts = jnp.where(lane == 3 * expert + piece, term, parts)
-                value = value - term
-        by_slot = dot(parts.astype(jnp.bfloat16), chosen, TN)
-        weight_rows = jnp.concatenate(
-            [
-                by_slot[0:1] + by_slot[1:2] + by_slot[2:3],
-                by_slot[3:4] + by_slot[4:5] + by_slot[5:6],
-                jnp.zeros((6, slots), jnp.float32),
-            ],
-            axis=0,
-        )
-        if turn == 0:
-            aux_in[0] = weight_rows
-        else:
-            aux_out[turn] = weight_rows
-            dispatch_aux(turn).start()
+        for part in range(2):
+            piece = picked[part * size : (part + 1) * size]
+            if turn == 0:
+                rows_in[2 * part] = piece
+                forward(part).start()
+            else:
+                q = {(1, 0): 2, (2, 0): 3, (2, 1): 4, (3, 0): 5, (3, 1): 6, (1, 1): 7}[turn, part]
+                outgoing[q] = piece
+                if q < 7:
+                    dispatch(q).start()
+    dispatch(7).start()
     for load in loads:
         load.wait()
 
+    def weigh():
+        few = few_rows()
+        lane_of = lax.broadcasted_iota(jnp.int32, (tokens, 128), 1)
+        ids, weights = few[:, :2].astype(jnp.int32), few[:, 2:4]
+        for turn in range(peers):
+            parts = jnp.zeros((tokens, 128), jnp.float32)
+            for expert in range(2):
+                name = 2 * group_of[turn] + expert
+                value = jnp.where(ids[:, :1] == name, weights[:, :1], 0.0) + jnp.where(
+                    ids[:, 1:2] == name, weights[:, 1:2], 0.0
+                )
+                for piece in range(3):
+                    term = value.astype(jnp.bfloat16).astype(jnp.float32)
+                    parts = jnp.where(lane_of == 3 * expert + piece, term, parts)
+                    value = value - term
+            by_slot = dot(
+                parts.astype(jnp.bfloat16), select[:, turn * slots : (turn + 1) * slots], TN
+            )
+            weight_rows = jnp.concatenate(
+                [
+                    by_slot[0:1] + by_slot[1:2] + by_slot[2:3],
+                    by_slot[3:4] + by_slot[4:5] + by_slot[5:6],
+                    jnp.zeros((6, slots), jnp.float32),
+                ],
+                axis=0,
+            )
+            if turn == 0:
+                factors[0] = as_columns(weight_rows)
+            else:
+                aux_out[turn] = weight_rows
+                dispatch_aux(turn).start()
+
     def step(t, carry):
         @pl.when(t < blocks)
         def _():
             k = t
-            turn = k // 2
-
-            @pl.when(jnp.logical_and(k % 2 == 0, k > 0))
+            q = k // 2
+
+            @pl.when(jnp.logical_and(k % 2 == 0, q > 1))
             def _():
-                dispatch(turn).wait_recv()
-                forward(turn).start()
+                dispatch(q).wait_recv()
+                forward(q).start()
 
             @pl.when(k % 2 == 1)
             def _():
-                forward(turn).wait_recv()
+                forward(q).wait_recv()
 
             block = rows_in[k]
             for part, columns in ((part_a, pl.ds(0, width)), (part_b, pl.ds(width, width))):
@@ -967,9 +1123,13 @@
             for copy in sum_first(k):
                 copy.start()
 
-        @pl.when(jnp.logical_and(t >= 1, t < blocks + 1))
-        def _():
-            k = t - 1
+        @pl.when(t == 1)
+        def _():
+            weigh()
+
+        @pl.when(jnp.logical_and(t >= LAG, t < blocks + LAG))
+        def _():
+            k = t - LAG
             copies = sum_first(k)
             nexts = sum_second(k)
             copies[0].wait_recv()
@@ -985,9 +1145,9 @@
             ).astype(jnp.bfloat16)
             nexts[1].start()
 
-        @pl.when(jnp.logical_and(t >= 2, t < blocks + 2))
-        def _():
-            k = t - 2
+        @pl.when(jnp.logical_and(t >= 2 * LAG, t < blocks + 2 * LAG))
+        def _():
+            k = t - 2 * LAG
             copies = sum_second(k)
             nexts = spread_first(k)
             for i, (part, first, second, hidden, major, minor) in enumerate(
@@ -1007,73 +1167,74 @@
                 hidden[k, mine] = (gate * sigmoid(gate) * up).astype(jnp.bfloat16)
                 nexts[i].start()
 
-        @pl.when(jnp.logical_and(t >= 3, t < blocks + 3))
-        def _():
-            k = t - 3
+        @pl.when(jnp.logical_and(t >= 3 * LAG, t < blocks + 3 * LAG))
+        def _():
+            k = t - 3 * LAG
             for copy, follow in zip(spread_first(k), spread_second(k)):
                 copy.wait_recv()
                 follow.start()
 
-        @pl.when(jnp.logical_and(t >= 4, t < blocks + 4))
-        def _():
-            k = t - 4
-            turn = k // 2
+        @pl.when(jnp.logical_and(t >= 4 * LAG, t < blocks + 4 * LAG))
+        def _():
+            k = t - 4 * LAG
+            q = k // 2
             for copy in spread_second(k):
                 copy.wait_recv()
             result = dot(hidden_a[k], down_w[:width, :], NN) + dot(hidden_b[k], down_w[width:, :], NN)
 
             @pl.when(k % 2 == 0)
             def _():
-                own_res[turn] = result
+                own_res[q] = result
 
             @pl.when(k % 2 == 1)
             def _():
-                pair_out[turn] = result.astype(jnp.bfloat16)
-                pair(turn).start()
-
-        @pl.when(jnp.logical_and(t >= 6, t % 2 == 0))
-        def _():
-            turn = (t - 6) // 2
-
-            @pl.when(turn > 0)
+                pair_out[q] = result.astype(jnp.bfloat16)
+                pair(q).start()
+
+        last = t - 5 * LAG - 1
+
+        @pl.when(jnp.logical_and(last >= 0, last % 2 == 0))
+        def _():
+            q = last // 2
+
+            @pl.when(q == 2)
             def _():
-                dispatch_aux(turn).wait_recv()
-
-            pair(turn).wait_recv()
-            columns = jnp.concatenate([aux_in[turn]] * (128 // 8), axis=0).T
+                for turn in range(1, peers):
+                    dispatch_aux(turn).wait_recv()
+                    factors[turn] = as_columns(aux_in[turn])
+
+            pair(q).wait_recv()
+            columns = factors[turn_of(q), pl.ds(pl.multiple_of(half_of(q) * size, size), size), :]
             low, high = columns[:, 0:1], columns[:, 1:2]
             mine = jnp.where(core == 0, low, high)
             other = jnp.where(core == 0, high, low)
-            both = (own_res[turn] * mine + pair_in[turn].astype(jnp.float32) * other).astype(
-                jnp.bfloat16
-            )
-
-            @pl.when(turn == 0)
+            both = (own_res[q] * mine + pair_in[q].astype(jnp.float32) * other).astype(jnp.bfloat16)
+
+            @pl.when(q < 2)
             def _():
-                back_in[0] = both
-
-            @pl.when(turn > 0)
+                back_in[back_rows(q), :] = both
+
+            @pl.when(q >= 2)
             def _():
-                back_out[turn] = both
-                give_back(turn).start()
+                back_out[q] = both
+                give_back(q).start()
 
         return carry
 
-    lax.fori_loop(0, blocks + 5, step, 0)
-    total = midway_ref[...].astype(jnp.float32)
-    for turn in range(peers):
-        if turn > 0:
-            give_back(turn).wait_recv()
-        total = total + dot(select[turn], back_in[turn], NN)
+    lax.fori_loop(0, blocks + 5 * LAG, step, 0)
+    for q in range(2, units):
+        give_back(q).wait_recv()
+    total = midway_ref[...].astype(jnp.float32) + dot(select[...], back_in[...], NN)
     out_ref[...] = total.astype(jnp.bfloat16)
 
-    for turn in range(peers):
-        forward(turn).wait_send()
-        pair(turn).wait_send()
-        if turn > 0:
-            dispatch(turn).wait_send()
-            dispatch_aux(turn).wait_send()
-            give_back(turn).wait_send()
+    for q in range(units):
+        forward(q).wait_send()
+        pair(q).wait_send()
+        if q > 1:
+            dispatch(q).wait_send()
+            give_back(q).wait_send()
+    for turn in range(1, peers):
+        dispatch_aux(turn).wait_send()
 
     def drain(k, carry):
         for copies in (sum_first(k), sum_second(k), spread_first(k), spread_second(k)):
@@ -1089,61 +1250,66 @@
     hidden = expert_gate.shape[2]
     half = hidden // 2
     slots = tokens // 2
-    quarter = slots // 4
+    size = slots // 2
+    quarter = size // 4
     peers = GROUPS
-    blocks = 2 * peers
+    units = 2 * peers
+    blocks = 2 * units
     bf = jnp.bfloat16
     whole = pl.BlockSpec(memory_space=pltpu.VMEM)
-    far = pl.BlockSpec(memory_space=pl.ANY)
+    far = pl.BlockSpec(memory_space=pltpu.HBM)
     dma = pltpu.SemaphoreType.DMA
     return pl.pallas_call(
         expert_kernel,
-        in_specs=[whole] * 4 + [far] * 3,
+        in_specs=[far] * 2 + [whole] * 2 + [far] * 3,
         out_specs=whole,
         out_shape=jax.ShapeDtypeStruct((tokens, features), bf),
         scratch_shapes=[
+            pltpu.VMEM((tokens, features), bf),
+            pltpu.VMEM((tokens, features), bf),
             pltpu.VMEM((features, hidden), bf),
             pltpu.VMEM((features, hidden), bf),
             pltpu.VMEM((hidden, features), bf),
-            pltpu.VMEM((peers, tokens, slots), bf),
-            pltpu.VMEM((peers, slots, features), bf),
+            pltpu.VMEM((tokens, peers * slots), bf),
+            pltpu.VMEM((units, size, features), bf),
+            pltpu.VMEM((peers, slots, slots), jnp.float32),
             pltpu.VMEM((peers, 8, slots), jnp.float32),
             pltpu.VMEM((peers, 8, slots), jnp.float32),
-            pltpu.VMEM((blocks, slots, features), bf),
-            pltpu.VMEM((blocks, slots, hidden), bf),
-            pltpu.VMEM((blocks, slots, hidden), bf),
-            pltpu.VMEM((blocks, slots // 2, hidden), bf),
-            pltpu.VMEM((blocks, slots // 2, hidden), bf),
+            pltpu.VMEM((blocks, size, features), bf),
+            pltpu.VMEM((blocks, size, hidden), bf),
+            pltpu.VMEM((blocks, size, hidden), bf),
+            pltpu.VMEM((blocks, size // 2, hidden), bf),
+            pltpu.VMEM((blocks, size // 2, hidden), bf),
             pltpu.VMEM((blocks, quarter, hidden), bf),
             pltpu.VMEM((blocks, quarter, hidden), bf),
             pltpu.VMEM((blocks, quarter, hidden), bf),
             pltpu.VMEM((blocks, quarter, hidden), bf),
-            pltpu.VMEM((blocks, slots, half), bf),
-            pltpu.VMEM((blocks, slots, half), bf),
-            pltpu.VMEM((peers, slots, features), jnp.float32),
-            pltpu.VMEM((peers, slots, features), bf),
-            pltpu.VMEM((peers, slots, features), bf),
-            pltpu.VMEM((peers, slots, features), bf),
-            pltpu.VMEM((peers, slots, features), bf),
-            dma((3,)),
+            pltpu.VMEM((blocks, size, half), bf),
+            pltpu.VMEM((blocks, size, half), bf),
+            pltpu.VMEM((units, size, features), jnp.float32),
+            pltpu.VMEM((units, size, features), bf),
+            pltpu.VMEM((units, size, features), bf),
+            pltpu.VMEM((units, size, features), bf),
+            pltpu.VMEM((peers * slots, features), bf),
+            dma((5,)),
+            dma((units,)),
+            dma((units,)),
             dma((peers,)),
             dma((peers,)),
-            dma((peers,)),
-            dma((peers,)),
-            dma((peers,)),
-            dma((peers,)),
+            dma((units,)),
+            dma((units,)),
             dma((8, blocks)),
             dma((8, blocks)),
-            dma((peers,)),
-            dma((peers,)),
-            dma((peers,)),
-            dma((peers,)),
+            dma((units,)),
+            dma((units,)),
+            dma((units,)),
+            dma((units,)),
         ],
         compiler_params=pltpu.CompilerParams(
-            collective_id=4, has_side_effects=True, vmem_limit_bytes=52 * 1024 * 1024
+            collective_id=4, has_side_effects=True, vmem_limit_bytes=66_900_000
         ),
         name="experts",
-    )(normed, midway, expert_ids, route_weight, expert_gate, expert_up, expert_down)
+    )(normed, midway, expert_ids.T, route_weight.T, expert_gate, expert_up, expert_down)
 
 
 def local(

time: 160 us -> 139 us (0.87)
  Pallas kernels: 156 us -> 137 us
  local copies, waits for them, and re-layouts: 4.49 us -> 1.87 us
    pallas_call x1, Pallas kernels: 67.6 us -> 54.6 us  [mixed_tokens(): pl.pallas_call(mixer_kernel, in_specs=[whole] * 9 + [pl.BlockSpec(memory_...]
    pallas_call x1, Pallas kernels: 88.1 us -> 81.9 us  [routed_experts(): pl.pallas_call(expert_kernel, in_specs=[far] * 2 + [whole] * 2 + [far] *...]
    unnamed x7 -> x1, local copies, waits for them, and re-layouts: 4.49 us -> 1.87 us
where the time goes in v3:
time: 139 us; the launch traced here: 138 us
  Pallas kernels  137 us (99%)
  local copies, waits for them, and re-layouts  1.87 us (1%)
    pallas_call x1, Pallas kernels, routed_experts(): pl.pallas_call(expert_kernel, in_specs=[far] * 2 + [whole] * 2 + [far] *...  81.9 us
    pallas_call x1, Pallas kernels, mixed_tokens(): pl.pallas_call(mixer_kernel, in_specs=[whole] * 9 + [pl.BlockSpec(memory_...  54.6 us

profile of v3, /device:TPU:0, one launch (start us, length us, event | category | flops | bytes accessed | tf_op | source)
XLA Modules:
  0.0 138.4 jit_solution(13250612718284466291)
XLA Ops:
  0.0 54.6 %mixer.1 = (bf16[256,1024]{1,0:T(8,128)(2,1)}, bf16[256,1024]{1,0:T(8,128)(2,1)}) custom-call(bf16[256,1024]{1,0:T(8,128)(2,1)} %r_ref.1, bf16[256,1024]{1,0:T(8,128)(2,1)} %k_ref.1, bf16[256,1024]{1,0:T(8,128)(2,1)} %v_ref.1, bf16[256,1024]{1,0:T(8,128)(2,1)} %d_ref.1, bf16[256,1024]{1,0:T(8,128)(2,1)} %a_ref.1, bf16[256,1024]{1,0:T(8,128)(2,1)} %gate_ref.1, ...), custom_call_target="tpu_custom_call" | custom-call | tf_op jit(solution)/shard_map/mixer/pallas_call | solution.py:827
  54.6 81.9 %experts.1 = bf16[256,1024]{1,0:T(8,128)(2,1)} custom-call(bf16[256,1024]{1,0:T(8,128)(2,1)} %get-tuple-element.7.normed_hbm, bf16[256,1024]{1,0:T(8,128)(2,1)} %get-tuple-element.8.midway_hbm, s32[2,256]{1,0:T(2,128)} %bitcast.6, f32[2,256]{1,0:T(2,128)} %bitcast.7, bf16[1,1024,1024]{2,1,0:T(8,128)(2,1)} %gate_hbm.1, bf16[1,1024,1024]{2,1,0:T(8,128)(2,1)} %up_hbm.1, ...), custom_call_target="tpu_custom_call" | custom-call | tf_op jit(solution)/shard_map/experts/pallas_call | solution.py:1262
  136.5 1.9 %copy.17 = bf16[256,1024]{1,0:T(8,128)(2,1)} copy(bf16[256,1024]{1,0:T(8,128)(2,1)} %experts.1) | data formatting | bytes 1048576

commit v4 on v3

--- a/solution.py
+++ b/solution.py
@@ -865,6 +865,7 @@
 
 
 LAG = 1
+LEAD = 1
 
 
 def expert_kernel(
@@ -1102,34 +1103,13 @@
                 dispatch_aux(turn).start()
 
     def step(t, carry):
-        @pl.when(t < blocks)
-        def _():
-            k = t
-            q = k // 2
-
-            @pl.when(jnp.logical_and(k % 2 == 0, q > 1))
-            def _():
-                dispatch(q).wait_recv()
-                forward(q).start()
-
-            @pl.when(k % 2 == 1)
-            def _():
-                forward(q).wait_recv()
-
-            block = rows_in[k]
-            for part, columns in ((part_a, pl.ds(0, width)), (part_b, pl.ds(width, width))):
-                part[k, :, :width] = dot(block, gate_w[:, columns], NN).astype(jnp.bfloat16)
-                part[k, :, width:] = dot(block, up_w[:, columns], NN).astype(jnp.bfloat16)
-            for copy in sum_first(k):
-                copy.start()
-
         @pl.when(t == 1)
         def _():
             weigh()
 
-        @pl.when(jnp.logical_and(t >= LAG, t < blocks + LAG))
-        def _():
-            k = t - LAG
+        @pl.when(jnp.logical_and(t >= LEAD + LAG, t < blocks + LEAD + LAG))
+        def _():
+            k = t - LEAD - LAG
             copies = sum_first(k)
             nexts = sum_second(k)
             copies[0].wait_recv()
@@ -1145,9 +1125,9 @@
             ).astype(jnp.bfloat16)
             nexts[1].start()
 
-        @pl.when(jnp.logical_and(t >= 2 * LAG, t < blocks + 2 * LAG))
-        def _():
-            k = t - 2 * LAG
+        @pl.when(jnp.logical_and(t >= LEAD + 2 * LAG, t < blocks + LEAD + 2 * LAG))
+        def _():
+            k = t - LEAD - 2 * LAG
             copies = sum_second(k)
             nexts = spread_first(k)
             for i, (part, first, second, hidden, major, minor) in enumerate(
@@ -1167,16 +1147,37 @@
                 hidden[k, mine] = (gate * sigmoid(gate) * up).astype(jnp.bfloat16)
                 nexts[i].start()
 
-        @pl.when(jnp.logical_and(t >= 3 * LAG, t < blocks + 3 * LAG))
-        def _():
-            k = t - 3 * LAG
+        @pl.when(jnp.logical_and(t >= LEAD + 3 * LAG, t < blocks + LEAD + 3 * LAG))
+        def _():
+            k = t - LEAD - 3 * LAG
             for copy, follow in zip(spread_first(k), spread_second(k)):
                 copy.wait_recv()
                 follow.start()
 
-        @pl.when(jnp.logical_and(t >= 4 * LAG, t < blocks + 4 * LAG))
-        def _():
-            k = t - 4 * LAG
+        @pl.when(t < blocks)
+        def _():
+            k = t
+            q = k // 2
+
+            @pl.when(jnp.logical_and(k % 2 == 0, q > 1))
+            def _():
+                dispatch(q).wait_recv()
+                forward(q).start()
+
+            @pl.when(k % 2 == 1)
+            def _():
+                forward(q).wait_recv()
+
+            block = rows_in[k]
+            for part, columns in ((part_a, pl.ds(0, width)), (part_b, pl.ds(width, width))):
+                part[k, :, :width] = dot(block, gate_w[:, columns], NN).astype(jnp.bfloat16)
+                part[k, :, width:] = dot(block, up_w[:, columns], NN).astype(jnp.bfloat16)
+            for copy in sum_first(k):
+                copy.start()
+
+        @pl.when(jnp.logical_and(t >= LEAD + 4 * LAG, t < blocks + LEAD + 4 * LAG))
+        def _():
+            k = t - LEAD - 4 * LAG
             q = k // 2
             for copy in spread_second(k):
                 copy.wait_recv()
@@ -1191,7 +1192,7 @@
                 pair_out[q] = result.astype(jnp.bfloat16)
                 pair(q).start()
 
-        last = t - 5 * LAG - 1
+        last = t - LEAD - 5 * LAG - 1
 
         @pl.when(jnp.logical_and(last >= 0, last % 2 == 0))
         def _():
@@ -1221,7 +1222,7 @@
 
         return carry
 
-    lax.fori_loop(0, blocks + 5 * LAG, step, 0)
+    lax.fori_loop(0, blocks + LEAD + 5 * LAG, step, 0)
     for q in range(2, units):
         give_back(q).wait_recv()
     total = midway_ref[...].astype(jnp.float32) + dot(select[...], back_in[...], NN)

time: 139 us -> 137 us (0.986)
  Pallas kernels: 137 us -> 135 us
    pallas_call x1, Pallas kernels: 81.9 us -> 80.3 us  [routed_experts(): pl.pallas_call(expert_kernel, in_specs=[far] * 2 + [whole] * 2 + [far] *...]
where the time goes in v4:
time: 137 us
  Pallas kernels  135 us (99%)
  local copies, waits for them, and re-layouts  1.87 us (1%)
    pallas_call x1, Pallas kernels, routed_experts(): pl.pallas_call(expert_kernel, in_specs=[far] * 2 + [whole] * 2 + [far] *...  80.3 us
    pallas_call x1, Pallas kernels, mixed_tokens(): pl.pallas_call(mixer_kernel, in_specs=[whole] * 9 + [pl.BlockSpec(memory_...  54.6 us

profile of v4, /device:TPU:0, one launch (start us, length us, event | category | flops | bytes accessed | tf_op | source)
XLA Modules:
  0.0 136.8 jit_solution(14023138788912781947)
XLA Ops:
  0.0 54.6 %mixer.1 = (bf16[256,1024]{1,0:T(8,128)(2,1)}, bf16[256,1024]{1,0:T(8,128)(2,1)}) custom-call(bf16[256,1024]{1,0:T(8,128)(2,1)} %r_ref.1, bf16[256,1024]{1,0:T(8,128)(2,1)} %k_ref.1, bf16[256,1024]{1,0:T(8,128)(2,1)} %v_ref.1, bf16[256,1024]{1,0:T(8,128)(2,1)} %d_ref.1, bf16[256,1024]{1,0:T(8,128)(2,1)} %a_ref.1, bf16[256,1024]{1,0:T(8,128)(2,1)} %gate_ref.1, ...), custom_call_target="tpu_custom_call" | custom-call | tf_op jit(solution)/shard_map/mixer/pallas_call | solution.py:827
  54.6 80.3 %experts.1 = bf16[256,1024]{1,0:T(8,128)(2,1)} custom-call(bf16[256,1024]{1,0:T(8,128)(2,1)} %get-tuple-element.7.normed_hbm, bf16[256,1024]{1,0:T(8,128)(2,1)} %get-tuple-element.8.midway_hbm, s32[2,256]{1,0:T(2,128)} %bitcast.6, f32[2,256]{1,0:T(2,128)} %bitcast.7, bf16[1,1024,1024]{2,1,0:T(8,128)(2,1)} %gate_hbm.1, bf16[1,1024,1024]{2,1,0:T(8,128)(2,1)} %up_hbm.1, ...), custom_call_target="tpu_custom_call" | custom-call | tf_op jit(solution)/shard_map/experts/pallas_call | solution.py:1263
  134.9 1.9 %copy.17 = bf16[256,1024]{1,0:T(8,128)(2,1)} copy(bf16[256,1024]{1,0:T(8,128)(2,1)} %experts.1) | data formatting | bytes 1048576

commit v5 on v4

--- a/solution.py
+++ b/solution.py
@@ -743,6 +743,10 @@
         def _():
             join(t - 1)
 
+        @pl.when(within(t - 3))
+        def _():
+            pass_on(t - 3)
+
         @pl.when(jnp.logical_and(z == 0, within(t - 1)))
         def _():
             finish(t - 1)
@@ -750,10 +754,6 @@
         @pl.when(jnp.logical_and(z > 0, within(t - 2)))
         def _():
             finish(t - 2)
-
-        @pl.when(within(t - 3))
-        def _():
-            pass_on(t - 3)
 
         @pl.when(within(t - 4))
         def _():

time: 137 us -> 136 us (level)
    pallas_call x1, Pallas kernels: 54.6 us -> 53.2 us  [mixed_tokens(): pl.pallas_call(mixer_kernel, in_specs=[whole] * 9 + [pl.BlockSpec(memory_...]
where the time goes in v5:
time: 136 us
  Pallas kernels  134 us (99%)
  local copies, waits for them, and re-layouts  1.87 us (1%)
    pallas_call x1, Pallas kernels, routed_experts(): pl.pallas_call(expert_kernel, in_specs=[far] * 2 + [whole] * 2 + [far] *...  80.8 us
    pallas_call x1, Pallas kernels, mixed_tokens(): pl.pallas_call(mixer_kernel, in_specs=[whole] * 9 + [pl.BlockSpec(memory_...  53.2 us

profile of v5, /device:TPU:0, one launch (start us, length us, event | category | flops | bytes accessed | tf_op | source)
XLA Modules:
  0.0 135.9 jit_solution(8520244277947866469)
XLA Ops:
  0.0 53.2 %mixer.1 = (bf16[256,1024]{1,0:T(8,128)(2,1)}, bf16[256,1024]{1,0:T(8,128)(2,1)}) custom-call(bf16[256,1024]{1,0:T(8,128)(2,1)} %r_ref.1, bf16[256,1024]{1,0:T(8,128)(2,1)} %k_ref.1, bf16[256,1024]{1,0:T(8,128)(2,1)} %v_ref.1, bf16[256,1024]{1,0:T(8,128)(2,1)} %d_ref.1, bf16[256,1024]{1,0:T(8,128)(2,1)} %a_ref.1, bf16[256,1024]{1,0:T(8,128)(2,1)} %gate_ref.1, ...), custom_call_target="tpu_custom_call" | custom-call | tf_op jit(solution)/shard_map/mixer/pallas_call | solution.py:827
  53.2 80.8 %experts.1 = bf16[256,1024]{1,0:T(8,128)(2,1)} custom-call(bf16[256,1024]{1,0:T(8,128)(2,1)} %get-tuple-element.7.normed_hbm, bf16[256,1024]{1,0:T(8,128)(2,1)} %get-tuple-element.8.midway_hbm, s32[2,256]{1,0:T(2,128)} %bitcast.6, f32[2,256]{1,0:T(2,128)} %bitcast.7, bf16[1,1024,1024]{2,1,0:T(8,128)(2,1)} %gate_hbm.1, bf16[1,1024,1024]{2,1,0:T(8,128)(2,1)} %up_hbm.1, ...), custom_call_target="tpu_custom_call" | custom-call | tf_op jit(solution)/shard_map/experts/pallas_call | solution.py:1263
  134.0 1.9 %copy.17 = bf16[256,1024]{1,0:T(8,128)(2,1)} copy(bf16[256,1024]{1,0:T(8,128)(2,1)} %experts.1) | data formatting | bytes 1048576
